TPU v7x, 512 devices: a whole 4x4x16 slice. The times are simulated.
512 devices in a mesh: sp: 128 (over z, x, core), tp: 4 (over y).
Axes of the slice: x: 4, y: 4, z: 16, core: 2. Of those that a mesh axis runs over, the one named last changes fastest.
Arguments:
- queries: bfloat16 [16384, 1024], P('sp', 'tp'), may hold values from -12 to 12
- keys: bfloat16 [16384, 256], P('sp', 'tp'), may hold values from -12 to 12
- values: bfloat16 [16384, 256], P('sp', 'tp'), may hold values from -6 to 6
- log_gate: float32 [16, 16384], P('tp', 'sp'), may hold values from -0.2 to 0, as said below
- log_sum: float32 [16, 16384], P('tp', 'sp'), may hold values from -100 to 100, as said below
- output: bfloat16 [16384, 1024], P('sp', 'tp'), may hold values from -6 to 6
- cotangent: bfloat16 [16384, 1024], P('sp', 'tp'), may hold values from -12 to 12
- normed: bfloat16 [16384, 2048], P('sp', 'tp'), may hold values from -24 to 24
Outputs:
- query_grad: bfloat16 [16384, 1024], P('sp', 'tp')
- key_grad: bfloat16 [16384, 256], P('sp', 'tp')
- value_grad: bfloat16 [16384, 256], P('sp', 'tp')
- weight_grad: float32 [2048, 256], P('sp', 'tp')
Inputs may be any that keep to these rules, and one draw needn't show every extreme that they name: `log_gate`: every entry is negative. log_sum[h, t] is the logarithm of the sum over s <= t of exp of the scores of the steps (before log_sum is subtracted), computed from the given queries, keys and log_gate.
All inputs are finite; a program needn't handle non-finite values.
Results may differ from a plain program's by a relative error of at most 0.005.
Values may be sent and summed in bfloat16 or wider, within the bound.
A program may use at most 64 MiB of HBM per device.

v0:
```python
import jax
import jax.numpy as jnp
from jax import lax
from jax.sharding import Mesh
from jax.sharding import PartitionSpec as P

HDIM = 64
SP = ("sp_0", "sp_1", "sp_2")


NEG_LARGE = -1e30


def nothing_yet(x, identity):
    return jnp.zeros_like(x) + jnp.asarray(identity, x.dtype)


def entering(x, axes, combine, identity):
    before = start = nothing_yet(x, identity)
    total = x
    for axis in reversed(axes):
        size, place = (lax.axis_size(axis), lax.axis_index(axis))
        pieces = lax.all_gather(total, axis)
        inside, total = (start, start)
        for k in range(size):
            passed = k < place
            total = combine(total, pieces[k])
            inside = jnp.where(passed, total, inside)
        before = combine(inside, before)
    return before


def shifted(x, axis, by):
    size = lax.axis_size(axis)
    pairs = [(i, i + by) for i in range(size) if 0 <= i + by < size]
    return lax.ppermute(x, axis, pairs)


def shifted_2(x, axis, by):
    size = lax.axis_size(axis)
    return lax.ppermute(x, axis, [(i, (i + by) % size) for i in range(size)])


def in_order(tiles, dim):
    tiles = jnp.moveaxis(tiles, 0, dim)
    dims = tiles.shape
    return tiles.reshape(*dims[:dim], dims[dim] * dims[dim + 1], *dims[dim + 2 :])


def copy_for_each(x, axis):
    size = lax.axis_size(axis)
    return lax.all_to_all(jnp.broadcast_to(x[None], (size, *x.shape)), axis, 0, 0, tiled=True)


def gathered_copies(x, axis, dim):
    return in_order(copy_for_each(x, axis), dim)


def own_block(tiles, axes, sequence):
    dims = [lax.axis_size(a) for a in axes]
    tiles = tiles.reshape(*dims, *tiles.shape[1:])
    tiles = tiles.transpose(*sequence, *range(len(axes), tiles.ndim))
    tiles = tiles.reshape(-1, *tiles.shape[len(axes) :])
    for k in sequence:
        tiles = lax.psum_scatter(tiles, axes[k], scatter_dimension=0, tiled=True)
    return tiles[0]


def cut_along(x, dim, size):
    dims = x.shape
    tiles = x.reshape(*dims[:dim], size, dims[dim] // size, *dims[dim + 1 :])
    return jnp.moveaxis(tiles, dim, 0)


def sum_by_axis(x, axes, sequence, dim):
    size = lax.axis_size(axes)
    return own_block(cut_along(x, dim, size), axes, sequence)


def add_pair(earlier, later):
    return earlier + later


def body(queries, keys, values, log_gate, log_sum, output, cotangent, normed):
    tokens = queries.shape[0]
    head_count = log_gate.shape[0]
    kv_width = keys.shape[1]
    kv_heads = kv_width // HDIM
    groups = head_count // kv_heads
    inverse_root = HDIM ** (-0.5)
    devices = lax.axis_size(SP)
    my_index = lax.axis_index(SP)
    depth = 8
    totals = jnp.sum(log_gate, axis=1)
    before = entering(totals, SP, add_pair, jnp.zeros_like(totals))
    cumulative = jnp.cumsum(log_gate, axis=1) + before[:, None]
    row_terms = jnp.sum(
        (output.astype(jnp.float32) * cotangent.astype(jnp.float32)).reshape(
            tokens, head_count, HDIM
        ),
        axis=2,
    ).T
    query_split = queries.reshape(tokens, kv_heads, groups, HDIM)
    cotan_split = cotangent.reshape(tokens, kv_heads, groups, HDIM)
    cum_rows = cumulative.reshape(kv_heads, groups, tokens)
    lse_rows = log_sum.reshape(kv_heads, groups, tokens)
    term_rows = row_terms.reshape(kv_heads, groups, tokens)
    positions = my_index * tokens + jnp.arange(tokens)
    last_row = my_index * tokens + tokens - 1

    def visit_bundle(bundle, bundle_cum, key_pos):
        count = bundle.shape[0]
        block_rows = bundle.shape[1]
        key_rows = count * block_rows
        flat = bundle.reshape(key_rows, 2 * kv_width)
        flat_cum = jnp.transpose(bundle_cum, (1, 0, 2)).reshape(kv_heads, groups, key_rows)
        flat_pos = key_pos.reshape(key_rows)
        key_part = flat[:, :kv_width].reshape(key_rows, kv_heads, HDIM)
        value_part = flat[:, kv_width:].reshape(key_rows, kv_heads, HDIM)

        def attend(unused):
            scores = (
                jnp.einsum(
                    "qhgd,khd->hgqk", query_split, key_part, preferred_element_type=jnp.float32
                )
                * inverse_root
            )
            scores = (
                scores + cum_rows[:, :, :, None] - flat_cum[:, :, None, :] - lse_rows[:, :, :, None]
            )
            allowed = flat_pos[None, :] <= positions[:, None]
            weights = jnp.exp(jnp.where(allowed, scores, NEG_LARGE))
            upstream = jnp.einsum(
                "qhgd,khd->hgqk", cotan_split, value_part, preferred_element_type=jnp.float32
            )
            dscore_low = (weights * (upstream - term_rows[:, :, :, None])).astype(jnp.bfloat16)
            weights_low = weights.astype(jnp.bfloat16)
            query_add = (
                jnp.einsum(
                    "hgqk,khd->qhgd", dscore_low, key_part, preferred_element_type=jnp.float32
                )
                * inverse_root
            )
            key_add = (
                jnp.einsum(
                    "hgqk,qhgd->khd", dscore_low, query_split, preferred_element_type=jnp.float32
                )
                * inverse_root
            )
            value_add = jnp.einsum(
                "hgqk,qhgd->khd", weights_low, cotan_split, preferred_element_type=jnp.float32
            )
            joined = jnp.concatenate(
                [key_add.reshape(key_rows, kv_width), value_add.reshape(key_rows, kv_width)], axis=1
            )
            return (query_add, joined.reshape(count, block_rows, 2 * kv_width))

        def nothing(unused):
            return (
                jnp.zeros((tokens, kv_heads, groups, HDIM), jnp.float32),
                jnp.zeros((count, block_rows, 2 * kv_width), jnp.float32),
            )

        return lax.cond(jnp.min(flat_pos) <= last_row, attend, nothing, 0)

    stacked = jnp.concatenate([keys, values], axis=1)
    query_start = jnp.zeros((tokens, kv_heads, groups, HDIM), jnp.float32)
    copies = jnp.arange(depth)
    turns = devices // depth
    bundle_pieces = [stacked]
    bundle_cums = [cumulative]
    for step in range(1, depth):
        bundle_pieces.append(shifted(stacked, SP, step))
        bundle_cums.append(shifted(cumulative, SP, step))

    def turn(turn_index, state_now):
        query_total, bundle, bundle_cum, bundle_grads = state_now
        anchor = (my_index - depth * turn_index) % devices
        blocks = (anchor - copies) % devices
        key_pos = blocks[:, None] * tokens + jnp.arange(tokens)[None, :]
        query_add, grad_add = visit_bundle(bundle, bundle_cum, key_pos)
        bundle = shifted(bundle, SP, depth)
        bundle_cum, bundle_grads = shifted_2((bundle_cum, bundle_grads + grad_add), SP, depth)
        return (query_total + query_add, bundle, bundle_cum, bundle_grads)

    start_state = (
        query_start,
        jnp.stack(bundle_pieces),
        jnp.stack(bundle_cums),
        jnp.zeros((depth, tokens, 2 * kv_width), jnp.float32),
    )
    finished = lax.fori_loop(0, turns, turn, start_state)
    query_total = finished[0]
    final_grads = finished[3]
    gradients = final_grads[0]
    for step in range(1, depth):
        gradients = gradients + shifted(final_grads[step], SP, -step)
    query_grad = query_total.reshape(tokens, head_count * HDIM).astype(jnp.bfloat16)
    key_grad = gradients[:, :kv_width].astype(jnp.bfloat16)
    value_grad = gradients[:, kv_width:].astype(jnp.bfloat16)
    whole_rows = gathered_copies(normed, "tp", 1)
    weight_grad = sum_by_axis(
        lax.dot_general(
            whole_rows, key_grad, (((0,), (0,)), ((), ())), preferred_element_type=jnp.float32
        ),
        SP,
        (2, 0, 1),
        0,
    )
    return (query_grad, key_grad, value_grad, weight_grad)


def solution(mesh):
    split = Mesh(mesh.devices.reshape(16, 4, 2, mesh.shape["tp"]), ("sp_0", "sp_1", "sp_2", "tp"))
    placed = (
        P(SP, "tp"),
        P(SP, "tp"),
        P(SP, "tp"),
        P("tp", SP),
        P("tp", SP),
        P(SP, "tp"),
        P(SP, "tp"),
        P(SP, "tp"),
    )
    return jax.shard_map(
        body,
        mesh=split,
        in_specs=placed,
        out_specs=(P(SP, "tp"), P(SP, "tp"), P(SP, "tp"), P(SP, "tp")),
        check_vma=False,
    )
```

profile of v0, /device:TPU:1, one launch (start us, length us, event | category | flops | bytes accessed | tf_op | source)
XLA Modules:
  0.0 637.4 jit_solution(11120356752376729763)
XLA Ops:
  11.2 8.9 %all-reduce = f32[8]{0:T(128)S(1)} all-reduce(f32[8]{0:T(128)S(1)} %dynamic-update-slice), channel_id=2, replica_groups=mesh['sp_0'=16,'sp_1'=4,'sp_2'=2,'tp'=4] {'sp_2'}, use_global_device_ids=true, to_apply=%add | all-reduce | flops 8 | bytes 64
  28.3 25.2 %all-gather.2 = f32[16,1,4]{2,1,0:T(1,128)S(1)} all-gather(f32[1,1,4]{2,1,0:T(1,128)S(1)} %fusion.51), channel_id=1, replica_groups=mesh['sp_0'=16,'sp_1'=4,'sp_2'=2,'tp'=4] {'sp_0'}, dimensions={0}, use_global_device_ids=true | all-gather | bytes 272 | tf_op jit(solution)/shard_map/all_gather | solution.py:23
  53.7 10.7 %collective-permute-start.10 = (f32[4,128]{1,0:T(4,128)S(1)}, f32[4,128]{1,0:T(4,128)S(1)}, u32[]{:S(2)}, u32[]{:S(2)}) collective-permute-start(f32[4,128]{1,0:T(4,128)S(1)} %broadcast_add_fusion.1), channel_id=1, source_target_pairs={{0,4},{4,8},{8,12},{12,16},{16,20},{20,24},{24,28},{28,32},{32,36}... | collective-permute-start | bytes 6152 | tf_op jit(solution)/shard_map/ppermute | solution.py:36
  115.6 332.4 %while.22 = (s32[]{:T(128)}, f32[128,1,4,64]{0,3,2,1:T(8,128)S(1)}, bf16[8,128,128]{1,0,2:T(8,128)(2,1)S(1)}, f32[8,4,128]{2,0,1:T(8,128)S(1)}, f32[8,128,128]{1...) while((s32[]{:T(128)}, f32[128,1,4,64]{0,3,2,1:T(8,128)S(1)}, ...), condition=%wide.region_7.8_spmd.clone, body=%wide.region_3.7_spmd.clone.sunk | while | flops 340822272 | bytes 19432036 | solution.py:192
  129.7 11.2 %collective-permute-done.1 = f32[8,4,128]{2,0,1:T(8,128)S(1)} collective-permute-done((f32[8,4,128]{2,0,1:T(8,128)S(1)}, f32[8,4,128]{2,0,1:T(8,128)S(1)}, u32[]{:S(2)}, u32[]{:S(2)}) %collective-permute-start.1) | collective-permute-done | bytes 16416 | tf_op jit(solution)/shard_map/while/body/eval_jaxpr/ppermute | solution.py:41
  142.5 7.0 %collective-permute-start.2 = (f32[8,128,128]{1,2,0:T(8,128)S(1)}, f32[8,128,128]{1,2,0:T(8,128)S(1)}, u32[]{:S(2)}, u32[]{:S(2)}) collective-permute-start(f32[8,128,128]{1,2,0:T(8,128)S(1)} %add.609), channel_id=1, source_target_pairs={{0,32},{4,36},{8,40},{12,44},{16,48},{20,52},{24,56},{28,60},{32,6... | collective-permute-start | bytes 1572872 | tf_op jit(solution)/shard_map/while/body/eval_jaxpr/ppermute | solution.py:41
  154.1 11.3 %collective-permute-done.1 = f32[8,4,128]{2,0,1:T(8,128)S(1)} collective-permute-done((f32[8,4,128]{2,0,1:T(8,128)S(1)}, f32[8,4,128]{2,0,1:T(8,128)S(1)}, u32[]{:S(2)}, u32[]{:S(2)}) %collective-permute-start.1) | collective-permute-done | bytes 16416 | tf_op jit(solution)/shard_map/while/body/eval_jaxpr/ppermute | solution.py:41
  179.0 7.3 %collective-permute-done.1 = f32[8,4,128]{2,0,1:T(8,128)S(1)} collective-permute-done((f32[8,4,128]{2,0,1:T(8,128)S(1)}, f32[8,4,128]{2,0,1:T(8,128)S(1)}, u32[]{:S(2)}, u32[]{:S(2)}) %collective-permute-start.1) | collective-permute-done | bytes 16416 | tf_op jit(solution)/shard_map/while/body/eval_jaxpr/ppermute | solution.py:41
  195.2 8.3 %collective-permute-start.1 = (f32[8,4,128]{2,0,1:T(8,128)S(1)}, f32[8,4,128]{2,0,1:T(8,128)S(1)}, u32[]{:S(2)}, u32[]{:S(2)}) collective-permute-start(f32[8,4,128]{2,0,1:T(8,128)S(1)} %copy.111), channel_id=1, source_target_pairs={{0,32},{4,36},{8,40},{12,44},{16,48},{20,52},{24,56},{28,60},{32,6... | collective-permute-start | bytes 49160 | tf_op jit(solution)/shard_map/while/body/eval_jaxpr/ppermute | solution.py:41
  212.1 6.8 %collective-permute-start = (bf16[8,128,128]{1,0,2:T(8,128)(2,1)S(1)}, bf16[8,128,128]{1,0,2:T(8,128)(2,1)S(1)}, u32[]{:S(2)}, u32[]{:S(2)}) collective-permute-start(bf16[8,128,128]{1,0,2:T(8,128)(2,1)S(1)} %copy.110), channel_id=1, source_target_pairs={{0,32},{4,36},{8,40},{12,44},{16,48},{20,52},{24,56},{28,60},{32,6... | collective-permute-start | bytes 786440 | tf_op jit(solution)/shard_map/while/body/eval_jaxpr/ppermute | solution.py:36
  265.9 6.7 %collective-permute-done.1 = f32[8,4,128]{2,0,1:T(8,128)S(1)} collective-permute-done((f32[8,4,128]{2,0,1:T(8,128)S(1)}, f32[8,4,128]{2,0,1:T(8,128)S(1)}, u32[]{:S(2)}, u32[]{:S(2)}) %collective-permute-start.1) | collective-permute-done | bytes 16416 | tf_op jit(solution)/shard_map/while/body/eval_jaxpr/ppermute | solution.py:41
  284.0 9.5 %collective-permute-done.1 = f32[8,4,128]{2,0,1:T(8,128)S(1)} collective-permute-done((f32[8,4,128]{2,0,1:T(8,128)S(1)}, f32[8,4,128]{2,0,1:T(8,128)S(1)}, u32[]{:S(2)}, u32[]{:S(2)}) %collective-permute-start.1) | collective-permute-done | bytes 16416 | tf_op jit(solution)/shard_map/while/body/eval_jaxpr/ppermute | solution.py:41
  301.3 12.7 %collective-permute-done.1 = f32[8,4,128]{2,0,1:T(8,128)S(1)} collective-permute-done((f32[8,4,128]{2,0,1:T(8,128)S(1)}, f32[8,4,128]{2,0,1:T(8,128)S(1)}, u32[]{:S(2)}, u32[]{:S(2)}) %collective-permute-start.1) | collective-permute-done | bytes 16416 | tf_op jit(solution)/shard_map/while/body/eval_jaxpr/ppermute | solution.py:41
  320.9 13.1 %collective-permute-done.1 = f32[8,4,128]{2,0,1:T(8,128)S(1)} collective-permute-done((f32[8,4,128]{2,0,1:T(8,128)S(1)}, f32[8,4,128]{2,0,1:T(8,128)S(1)}, u32[]{:S(2)}, u32[]{:S(2)}) %collective-permute-start.1) | collective-permute-done | bytes 16416 | tf_op jit(solution)/shard_map/while/body/eval_jaxpr/ppermute | solution.py:41
  340.9 12.3 %collective-permute-done.1 = f32[8,4,128]{2,0,1:T(8,128)S(1)} collective-permute-done((f32[8,4,128]{2,0,1:T(8,128)S(1)}, f32[8,4,128]{2,0,1:T(8,128)S(1)}, u32[]{:S(2)}, u32[]{:S(2)}) %collective-permute-start.1) | collective-permute-done | bytes 16416 | tf_op jit(solution)/shard_map/while/body/eval_jaxpr/ppermute | solution.py:41
  360.1 11.4 %collective-permute-done.1 = f32[8,4,128]{2,0,1:T(8,128)S(1)} collective-permute-done((f32[8,4,128]{2,0,1:T(8,128)S(1)}, f32[8,4,128]{2,0,1:T(8,128)S(1)}, u32[]{:S(2)}, u32[]{:S(2)}) %collective-permute-start.1) | collective-permute-done | bytes 16416 | tf_op jit(solution)/shard_map/while/body/eval_jaxpr/ppermute | solution.py:41
  378.4 10.8 %collective-permute-done.1 = f32[8,4,128]{2,0,1:T(8,128)S(1)} collective-permute-done((f32[8,4,128]{2,0,1:T(8,128)S(1)}, f32[8,4,128]{2,0,1:T(8,128)S(1)}, u32[]{:S(2)}, u32[]{:S(2)}) %collective-permute-start.1) | collective-permute-done | bytes 16416 | tf_op jit(solution)/shard_map/while/body/eval_jaxpr/ppermute | solution.py:41
  396.2 11.6 %collective-permute-done.1 = f32[8,4,128]{2,0,1:T(8,128)S(1)} collective-permute-done((f32[8,4,128]{2,0,1:T(8,128)S(1)}, f32[8,4,128]{2,0,1:T(8,128)S(1)}, u32[]{:S(2)}, u32[]{:S(2)}) %collective-permute-start.1) | collective-permute-done | bytes 16416 | tf_op jit(solution)/shard_map/while/body/eval_jaxpr/ppermute | solution.py:41
  415.2 11.9 %collective-permute-done.1 = f32[8,4,128]{2,0,1:T(8,128)S(1)} collective-permute-done((f32[8,4,128]{2,0,1:T(8,128)S(1)}, f32[8,4,128]{2,0,1:T(8,128)S(1)}, u32[]{:S(2)}, u32[]{:S(2)}) %collective-permute-start.1) | collective-permute-done | bytes 16416 | tf_op jit(solution)/shard_map/while/body/eval_jaxpr/ppermute | solution.py:41
  438.3 9.7 %collective-permute-done.1 = f32[8,4,128]{2,0,1:T(8,128)S(1)} collective-permute-done((f32[8,4,128]{2,0,1:T(8,128)S(1)}, f32[8,4,128]{2,0,1:T(8,128)S(1)}, u32[]{:S(2)}, u32[]{:S(2)}) %collective-permute-start.1) | collective-permute-done | bytes 16416 | tf_op jit(solution)/shard_map/while/body/eval_jaxpr/ppermute | solution.py:41
  448.0 30.2 %collective-permute-start.17 = (f32[128,128]{0,1:T(8,128)S(1)}, f32[128,128]{0,1:T(8,128)S(1)}, u32[]{:S(2)}, u32[]{:S(2)}) collective-permute-start(f32[128,128]{0,1:T(8,128)S(1)} %get-tuple-element.539), channel_id=1, source_target_pairs={{4,0},{8,4},{12,8},{16,12},{20,16},{24,20},{28,24},{32,28},{36,32}... | collective-permute-start | bytes 196616 | tf_op jit(solution)/shard_map/ppermute | solution.py:36
  502.5 28.5 %reduce-scatter.4.cloned.1.call-done = f32[64,16,64]{2,1,0:T(8,128)} async-done(((f32[128,16,64]{2,1,0:T(8,128)}), f32[64,16,64]{2,1,0:T(8,128)}) %reduce-scatter.4.cloned.1.call-update) | async-done | bytes 262160 | tf_op jit(solution)/shard_map/reduce_scatter | solution.py:65
  531.1 61.3 %reduce-scatter.6.cloned.1.call-done = f32[4,16,64]{2,1,0:T(8,128)} async-done(((f32[64,16,64]{2,1,0:T(8,128)}), f32[4,16,64]{2,1,0:T(8,128)}) %reduce-scatter.6.cloned.1.call-update) | async-done | bytes 16400 | tf_op jit(solution)/shard_map/reduce_scatter | solution.py:65
  593.2 37.7 %reduce-scatter.8.cloned.1.call-done = f32[1,16,64]{2,1,0:T(8,128)} async-done(((f32[4,16,64]{2,1,0:T(8,128)}), f32[1,16,64]{2,1,0:T(8,128)}) %reduce-scatter.8.cloned.1.call-update) | async-done | bytes 4112 | tf_op jit(solution)/shard_map/reduce_scatter | solution.py:65
  (352 shorter events, 248.8 us)
Async XLA Ops:
  53.7 30.0 %collective-permute-start.10 = (f32[4,128]{1,0:T(4,128)S(1)}, f32[4,128]{1,0:T(4,128)S(1)}, u32[]{:S(2)}, u32[]{:S(2)}) collective-permute-start(f32[4,128]{1,0:T(4,128)S(1)} %broadcast_add_fusion.1), channel_id=1, source_target_pairs={{0,4},{4,8},{8,12},{12,16},{16,20},{20,24},{24,28},{28,32},{32,36}... | collective-permute-start | bytes 6152 | tf_op jit(solution)/shard_map/ppermute | solution.py:36
  64.4 20.7 %collective-permute-start.11 = (f32[4,128]{1,0:T(4,128)S(1)}, f32[4,128]{1,0:T(4,128)S(1)}, u32[]{:S(2)}, u32[]{:S(2)}) collective-permute-start(f32[4,128]{1,0:T(4,128)S(1)} %broadcast_add_fusion.1), channel_id=1, source_target_pairs={{0,8},{4,12},{8,16},{12,20},{16,24},{20,28},{24,32},{28,36},{32,40... | collective-permute-start | bytes 6152 | tf_op jit(solution)/shard_map/ppermute | solution.py:36
  67.3 20.1 %collective-permute-start.12 = (f32[4,128]{1,0:T(4,128)S(1)}, f32[4,128]{1,0:T(4,128)S(1)}, u32[]{:S(2)}, u32[]{:S(2)}) collective-permute-start(f32[4,128]{1,0:T(4,128)S(1)} %broadcast_add_fusion.1), channel_id=1, source_target_pairs={{0,12},{4,16},{8,20},{12,24},{16,28},{20,32},{24,36},{28,40},{32,4... | collective-permute-start | bytes 6152 | tf_op jit(solution)/shard_map/ppermute | solution.py:36
  69.9 20.7 %collective-permute-start.13 = (f32[4,128]{1,0:T(4,128)S(1)}, f32[4,128]{1,0:T(4,128)S(1)}, u32[]{:S(2)}, u32[]{:S(2)}) collective-permute-start(f32[4,128]{1,0:T(4,128)S(1)} %broadcast_add_fusion.1), channel_id=1, source_target_pairs={{0,16},{4,20},{8,24},{12,28},{16,32},{20,36},{24,40},{28,44},{32,4... | collective-permute-start | bytes 6152 | tf_op jit(solution)/shard_map/ppermute | solution.py:36
  87.4 17.6 %collective-permute-start.3 = (bf16[128,128]{1,0:T(8,128)(2,1)S(1)}, bf16[128,128]{1,0:T(8,128)(2,1)S(1)}, u32[]{:S(2)}, u32[]{:S(2)}) collective-permute-start(bf16[128,128]{1,0:T(8,128)(2,1)S(1)} %get-tuple-element.534), channel_id=1, source_target_pairs={{0,4},{4,8},{8,12},{12,16},{16,20},{20,24},{24,28},{28,32},{32,36}... | collective-permute-start | bytes 98312 | tf_op jit(solution)/shard_map/ppermute | solution.py:36
  90.5 17.5 %collective-permute-start.4 = (bf16[128,128]{1,0:T(8,128)(2,1)S(1)}, bf16[128,128]{1,0:T(8,128)(2,1)S(1)}, u32[]{:S(2)}, u32[]{:S(2)}) collective-permute-start(bf16[128,128]{1,0:T(8,128)(2,1)S(1)} %get-tuple-element.534), channel_id=1, source_target_pairs={{0,8},{4,12},{8,16},{12,20},{16,24},{20,28},{24,32},{28,36},{32,40... | collective-permute-start | bytes 98312 | tf_op jit(solution)/shard_map/ppermute | solution.py:36
  95.6 18.7 %collective-permute-start.5 = (bf16[128,128]{1,0:T(8,128)(2,1)S(1)}, bf16[128,128]{1,0:T(8,128)(2,1)S(1)}, u32[]{:S(2)}, u32[]{:S(2)}) collective-permute-start(bf16[128,128]{1,0:T(8,128)(2,1)S(1)} %get-tuple-element.534), channel_id=1, source_target_pairs={{0,12},{4,16},{8,20},{12,24},{16,28},{20,32},{24,36},{28,40},{32,4... | collective-permute-start | bytes 98312 | tf_op jit(solution)/shard_map/ppermute | solution.py:36
  120.2 20.6 %collective-permute-start.2 = (f32[8,128,128]{1,2,0:T(8,128)S(1)}, f32[8,128,128]{1,2,0:T(8,128)S(1)}, u32[]{:S(2)}, u32[]{:S(2)}) collective-permute-start(f32[8,128,128]{1,2,0:T(8,128)S(1)} %add.609), channel_id=1, source_target_pairs={{0,32},{4,36},{8,40},{12,44},{16,48},{20,52},{24,56},{28,60},{32,6... | collective-permute-start | bytes 1572872 | tf_op jit(solution)/shard_map/while/body/eval_jaxpr/ppermute | solution.py:41
  142.5 22.9 %collective-permute-start.2 = (f32[8,128,128]{1,2,0:T(8,128)S(1)}, f32[8,128,128]{1,2,0:T(8,128)S(1)}, u32[]{:S(2)}, u32[]{:S(2)}) collective-permute-start(f32[8,128,128]{1,2,0:T(8,128)S(1)} %add.609), channel_id=1, source_target_pairs={{0,32},{4,36},{8,40},{12,44},{16,48},{20,52},{24,56},{28,60},{32,6... | collective-permute-start | bytes 1572872 | tf_op jit(solution)/shard_map/while/body/eval_jaxpr/ppermute | solution.py:41
  167.1 19.1 %collective-permute-start.2 = (f32[8,128,128]{1,2,0:T(8,128)S(1)}, f32[8,128,128]{1,2,0:T(8,128)S(1)}, u32[]{:S(2)}, u32[]{:S(2)}) collective-permute-start(f32[8,128,128]{1,2,0:T(8,128)S(1)} %add.609), channel_id=1, source_target_pairs={{0,32},{4,36},{8,40},{12,44},{16,48},{20,52},{24,56},{28,60},{32,6... | collective-permute-start | bytes 1572872 | tf_op jit(solution)/shard_map/while/body/eval_jaxpr/ppermute | solution.py:41
  188.0 18.3 %collective-permute-start.2 = (f32[8,128,128]{1,2,0:T(8,128)S(1)}, f32[8,128,128]{1,2,0:T(8,128)S(1)}, u32[]{:S(2)}, u32[]{:S(2)}) collective-permute-start(f32[8,128,128]{1,2,0:T(8,128)S(1)} %add.609), channel_id=1, source_target_pairs={{0,32},{4,36},{8,40},{12,44},{16,48},{20,52},{24,56},{28,60},{32,6... | collective-permute-start | bytes 1572872 | tf_op jit(solution)/shard_map/while/body/eval_jaxpr/ppermute | solution.py:41
  207.9 20.3 %collective-permute-start.2 = (f32[8,128,128]{1,2,0:T(8,128)S(1)}, f32[8,128,128]{1,2,0:T(8,128)S(1)}, u32[]{:S(2)}, u32[]{:S(2)}) collective-permute-start(f32[8,128,128]{1,2,0:T(8,128)S(1)} %add.609), channel_id=1, source_target_pairs={{0,32},{4,36},{8,40},{12,44},{16,48},{20,52},{24,56},{28,60},{32,6... | collective-permute-start | bytes 1572872 | tf_op jit(solution)/shard_map/while/body/eval_jaxpr/ppermute | solution.py:41
  230.0 21.0 %collective-permute-start.2 = (f32[8,128,128]{1,2,0:T(8,128)S(1)}, f32[8,128,128]{1,2,0:T(8,128)S(1)}, u32[]{:S(2)}, u32[]{:S(2)}) collective-permute-start(f32[8,128,128]{1,2,0:T(8,128)S(1)} %add.609), channel_id=1, source_target_pairs={{0,32},{4,36},{8,40},{12,44},{16,48},{20,52},{24,56},{28,60},{32,6... | collective-permute-start | bytes 1572872 | tf_op jit(solution)/shard_map/while/body/eval_jaxpr/ppermute | solution.py:41
  252.6 20.1 %collective-permute-start.2 = (f32[8,128,128]{1,2,0:T(8,128)S(1)}, f32[8,128,128]{1,2,0:T(8,128)S(1)}, u32[]{:S(2)}, u32[]{:S(2)}) collective-permute-start(f32[8,128,128]{1,2,0:T(8,128)S(1)} %add.609), channel_id=1, source_target_pairs={{0,32},{4,36},{8,40},{12,44},{16,48},{20,52},{24,56},{28,60},{32,6... | collective-permute-start | bytes 1572872 | tf_op jit(solution)/shard_map/while/body/eval_jaxpr/ppermute | solution.py:41
  274.3 19.2 %collective-permute-start.2 = (f32[8,128,128]{1,2,0:T(8,128)S(1)}, f32[8,128,128]{1,2,0:T(8,128)S(1)}, u32[]{:S(2)}, u32[]{:S(2)}) collective-permute-start(f32[8,128,128]{1,2,0:T(8,128)S(1)} %add.609), channel_id=1, source_target_pairs={{0,32},{4,36},{8,40},{12,44},{16,48},{20,52},{24,56},{28,60},{32,6... | collective-permute-start | bytes 1572872 | tf_op jit(solution)/shard_map/while/body/eval_jaxpr/ppermute | solution.py:41
  295.3 18.7 %collective-permute-start.2 = (f32[8,128,128]{1,2,0:T(8,128)S(1)}, f32[8,128,128]{1,2,0:T(8,128)S(1)}, u32[]{:S(2)}, u32[]{:S(2)}) collective-permute-start(f32[8,128,128]{1,2,0:T(8,128)S(1)} %add.609), channel_id=1, source_target_pairs={{0,32},{4,36},{8,40},{12,44},{16,48},{20,52},{24,56},{28,60},{32,6... | collective-permute-start | bytes 1572872 | tf_op jit(solution)/shard_map/while/body/eval_jaxpr/ppermute | solution.py:41
  315.7 18.4 %collective-permute-start.2 = (f32[8,128,128]{1,2,0:T(8,128)S(1)}, f32[8,128,128]{1,2,0:T(8,128)S(1)}, u32[]{:S(2)}, u32[]{:S(2)}) collective-permute-start(f32[8,128,128]{1,2,0:T(8,128)S(1)} %add.609), channel_id=1, source_target_pairs={{0,32},{4,36},{8,40},{12,44},{16,48},{20,52},{24,56},{28,60},{32,6... | collective-permute-start | bytes 1572872 | tf_op jit(solution)/shard_map/while/body/eval_jaxpr/ppermute | solution.py:41
  335.7 17.5 %collective-permute-start.2 = (f32[8,128,128]{1,2,0:T(8,128)S(1)}, f32[8,128,128]{1,2,0:T(8,128)S(1)}, u32[]{:S(2)}, u32[]{:S(2)}) collective-permute-start(f32[8,128,128]{1,2,0:T(8,128)S(1)} %add.609), channel_id=1, source_target_pairs={{0,32},{4,36},{8,40},{12,44},{16,48},{20,52},{24,56},{28,60},{32,6... | collective-permute-start | bytes 1572872 | tf_op jit(solution)/shard_map/while/body/eval_jaxpr/ppermute | solution.py:41
  409.4 17.7 %collective-permute-start.2 = (f32[8,128,128]{1,2,0:T(8,128)S(1)}, f32[8,128,128]{1,2,0:T(8,128)S(1)}, u32[]{:S(2)}, u32[]{:S(2)}) collective-permute-start(f32[8,128,128]{1,2,0:T(8,128)S(1)} %add.609), channel_id=1, source_target_pairs={{0,32},{4,36},{8,40},{12,44},{16,48},{20,52},{24,56},{28,60},{32,6... | collective-permute-start | bytes 1572872 | tf_op jit(solution)/shard_map/while/body/eval_jaxpr/ppermute | solution.py:41
  428.8 19.2 %collective-permute-start.2 = (f32[8,128,128]{1,2,0:T(8,128)S(1)}, f32[8,128,128]{1,2,0:T(8,128)S(1)}, u32[]{:S(2)}, u32[]{:S(2)}) collective-permute-start(f32[8,128,128]{1,2,0:T(8,128)S(1)} %add.609), channel_id=1, source_target_pairs={{0,32},{4,36},{8,40},{12,44},{16,48},{20,52},{24,56},{28,60},{32,6... | collective-permute-start | bytes 1572872 | tf_op jit(solution)/shard_map/while/body/eval_jaxpr/ppermute | solution.py:41
  448.0 35.4 %collective-permute-start.17 = (f32[128,128]{0,1:T(8,128)S(1)}, f32[128,128]{0,1:T(8,128)S(1)}, u32[]{:S(2)}, u32[]{:S(2)}) collective-permute-start(f32[128,128]{0,1:T(8,128)S(1)} %get-tuple-element.539), channel_id=1, source_target_pairs={{4,0},{8,4},{12,8},{16,12},{20,16},{24,20},{28,24},{32,28},{36,32}... | collective-permute-start | bytes 196616 | tf_op jit(solution)/shard_map/ppermute | solution.py:36
  491.7 39.3 %reduce-scatter.4.cloned.1.call-start = ((), (), s32[]{:S(2)}) async-start(), calls=%async_computation.4 | async-start | bytes 1572864 | tf_op jit(solution)/shard_map/reduce_scatter | solution.py:65
  502.4 90.0 %reduce-scatter.6.cloned.1.call-start = ((), (), s32[]{:S(2)}) async-start(), calls=%async_computation.5 | async-start | bytes 557056 | tf_op jit(solution)/shard_map/reduce_scatter | solution.py:65
  531.0 99.9 %reduce-scatter.8.cloned.1.call-start = ((), (), s32[]{:S(2)}) async-start(), calls=%async_computation.6 | async-start | bytes 40960 | tf_op jit(solution)/shard_map/reduce_scatter | solution.py:65
  (52 other events, 1170.8 us)
Sparse Core Ops, SparseCore 0:
  502.6 28.4 reduce-scatter.3
  533.8 58.5 reduce-scatter.5
  595.8 35.0 reduce-scatter.7
where the time goes:
time: 641 us; the launch traced here: 637 us
  waiting for transfers between devices  288 us (45%)
  starting transfers between devices  248 us (39%)
  blocking collectives  40.2 us (6%)
  other arithmetic  16.9 us (3%)
  between operations  15.6 us (2%)
  loops' own time  12.9 us (2%)
  local copies, waits for them, and re-layouts  12.7 us (2%)
    ppermute x32, waiting for transfers between devices, shifted_2(): return lax.ppermute(x, axis, [(i, (i + by) % size) for i in range(size)])  150 us
    ppermute x37, starting transfers between devices, shifted(): return lax.ppermute(x, axis, pairs)  137 us
    reduce_scatter x3, waiting for transfers between devices, own_block(): tiles = lax.psum_scatter(tiles, axes[k], scatter_dimension=0, tiled=True)  128 us
    ppermute x32, starting transfers between devices, shifted_2(): return lax.ppermute(x, axis, [(i, (i + by) % size) for i in range(size)])  108 us
    all_gather x1, blocking collectives, entering(): pieces = lax.all_gather(total, axis)  25.2 us
    unnamed x2, blocking collectives  15 us
  transfers between devices with their start and end apart: 73, of which 25 were waited for; matrix products, arithmetic and copies ran while one was open for 1% of the time, Pallas kernels for 0%

commit v1 on v0

v1 whole, which is shorter than its diff:
```python
import functools
import math

import jax
import jax.numpy as jnp
from jax import lax
from jax.experimental import pallas as pl
from jax.experimental.pallas import tpu as pltpu
from jax.sharding import Mesh
from jax.sharding import PartitionSpec as P

SP = ("sp_0", "sp_1", "sp_2")
MESH = pl.DeviceIdType.MESH
LOG2E = math.log2(math.e)
NEG_LARGE = -1e30
TOK = 128
TQ = 256
F32, BF16 = jnp.float32, jnp.bfloat16


def at(z=None, x=None, c=None, y=None):
    named = {"sp_0": z, "sp_1": x, "sp_2": c, "tp": y}
    return {k: v for k, v in named.items() if v is not None}


def greet(peers):
    barrier = pltpu.get_barrier_semaphore()
    for peer in peers:
        pl.semaphore_signal(barrier, inc=1, device_id=peer, device_id_type=MESH)
    pl.semaphore_wait(barrier, len(peers))


def remote(src, dst, send, recv, peer):
    return pltpu.make_async_remote_copy(
        src_ref=src, dst_ref=dst, send_sem=send, recv_sem=recv, device_id=peer, device_id_type=MESH
    )


def attention_kernel(
    nz, nx, ny,
    q_ref, k_ref, gate_ref, lse_ref, out_ref, do_ref, norm_ref,
    dq_out, dkv_out, norm_out,
    qg, dg, kv, aux, stat, kaux, ck, rowb, qtl, dtl, ktile, vtile, kcat, dq, dkvt, own,
    gsend, grecv, dqd, dqs, dqr,
    aux_s, aux_r, q_s, q_r, f_s, k_s, k_r, ka_s, ka_r, n_s, n_r, g_s, g_r, d_s, d_r, e_s, e_r,
):
    z, x, c, y = (lax.axis_index(a) for a in ("sp_0", "sp_1", "sp_2", "tp"))
    nb = 2 * nx
    b = 2 * x + c
    sib = at(c=1 - c)
    c1 = 0.125 * LOG2E

    def xc(r):
        k = lax.rem(b + r, nb)
        return at(x=k // 2, c=lax.rem(k, 2))

    def zz(r):
        return at(z=lax.rem(z + r, nz))

    def yy(r):
        return at(y=lax.rem(y + r, ny))

    gates = gate_ref[...]
    lane = lax.broadcasted_iota(jnp.int32, (4, TOK), 1)
    run = gates
    for s in (1, 2, 4, 8, 16, 32, 64):
        run = run + jnp.where(lane >= s, pltpu.roll(run, s, 1), 0.0)
    prod = (out_ref[...].astype(F32) * do_ref[...].astype(F32)).T
    terms = jnp.sum(prod.reshape(4, 64, TOK), axis=1)
    aux[b, 0:4, :] = run
    aux[b, 4:8, :] = run - lse_ref[...]
    aux[b, 8:12, :] = terms
    aux[b, 12:16, :] = jnp.zeros((4, TOK), F32)
    qg[b] = q_ref[...]
    dg[b] = do_ref[...]
    kv[z] = k_ref[...]

    greet([xc(r) for r in range(1, nb)] + [zz(r) for r in range(1, nz)] + [yy(r) for r in range(1, ny)])

    for r in range(1, nb):
        remote(aux.at[b], aux.at[b], aux_s.at[r], aux_r.at[b], xc(r)).start()
    for i, (src, dst) in enumerate(((q_ref, qg), (do_ref, dg))):
        remote(src, dst.at[b], f_s.at[i, x], q_r.at[i, b], sib).start()
    xorder = [r for pair in zip(range(1, nx // 2 + 1), range(nx - 1, nx // 2 - 1, -1)) for r in pair]
    xorder = list(dict.fromkeys(xorder))
    for r in xorder:
        peer = lax.rem(x + r, nx)
        for i, (src, dst) in enumerate(((q_ref, qg), (do_ref, dg))):
            remote(src, dst.at[b], q_s.at[i, r], q_r.at[i, b], at(x=peer)).start()
    zorder = [r for pair in zip(range(1, nz // 2 + 1), range(nz - 1, nz // 2 - 1, -1)) for r in pair]
    zorder = list(dict.fromkeys(zorder))

    def k_copy(r, peer):
        return remote(k_ref, kv.at[z], k_s.at[r], k_r.at[z], at(z=peer))

    def ka_copy(r, peer):
        return remote(kaux.at[z], kaux.at[z], ka_s.at[r], ka_r.at[z], at(z=peer))

    for r in zorder:
        peer = lax.rem(z + r, nz)

        @pl.when(peer > z)
        def _():
            k_copy(r, peer).start()

    for r in range(1, ny):
        remote(norm_ref, norm_out.at[y], n_s.at[r], n_r.at[y], yy(r)).start()
    norm_out[y] = norm_ref[...]

    for r in range(1, nb):
        k = lax.rem(b + r, nb)
        remote(aux.at[k], aux.at[k], aux_s.at[r], aux_r.at[k], xc(r)).wait_recv()
    before = jnp.zeros((4, TOK), F32)
    mine = jnp.zeros((4, TOK), F32)
    for k in range(nb):
        mine = jnp.where(b == k, before, mine)
        stat[k, 0:4, :] = (aux[k, 4:8, :] + before) * LOG2E
        stat[k, 4:8, :] = aux[k, 8:12, :]
        before = before + jnp.broadcast_to(aux[k, 0:4, TOK - 1 : TOK], (4, TOK))
    kaux[z, 0:4, :] = run + mine
    kaux[z, 4:8, :] = before

    for r in zorder:
        peer = lax.rem(z + r, nz)

        @pl.when(peer > z)
        def _():
            ka_copy(r, peer).start()

    for r in xorder:
        k = 2 * lax.rem(x + nx - r, nx) + c
        for i, dst in enumerate((qg, dg)):
            remote(dst.at[k], dst.at[k], q_s.at[i, 0], q_r.at[i, k], sib).wait_recv()
            remote(dst.at[k], dst.at[k], f_s.at[i, lax.rem(x + nx - r, nx)], q_r.at[i, k], sib).start()

    def offsets(i, total):
        k = z - 1 - i
        remote(kaux.at[k], kaux.at[k], ka_s.at[0], ka_r.at[k], sib).wait_recv()
        total = total + kaux[k, 4:8, :]
        ck[k, 0:4, :] = (kaux[k, 0:4, :] - total) * LOG2E
        return total

    ck[z, 0:4, :] = (run + mine) * LOG2E
    lax.fori_loop(0, z, offsets, jnp.zeros((4, TOK), F32))

    for k in range(nx):
        slot = 2 * k + 1 - c
        for i, dst in enumerate((qg, dg)):
            remote(dst.at[slot], dst.at[slot], q_s.at[i, 0], q_r.at[i, slot], sib).wait_recv()

    tb = TQ // TOK
    nt = nb // tb

    def prepare(k, _):
        t, i = k // tb, lax.rem(k, tb)
        qt = qg[k].T
        dt = dg[k].T
        stats = jnp.concatenate([stat[k], jnp.zeros((TOK - 8, TOK), F32)], 0).T
        for h in range(4):
            for j in range(tb):
                @pl.when(i == j)
                def _():
                    qtl[t, :, h * TQ + j * TOK : h * TQ + (j + 1) * TOK] = qt[64 * h : 64 * h + 64]
                    dtl[t, :, h * TQ + j * TOK : h * TQ + (j + 1) * TOK] = dt[64 * h : 64 * h + 64]
        for r in range(8):
            rowb[r, k] = jnp.broadcast_to(stats[:, r : r + 1], (TOK, TOK))
        dq[k] = jnp.zeros((TOK, 256), F32)
        return 0

    lax.fori_loop(0, nb, prepare, 0)

    even = lax.rem(z, 2) == 1
    skip = jnp.where(even, 0, 1)
    straight = jnp.minimum(nz - 1 - z, z)
    lane2 = lax.broadcasted_iota(jnp.int32, (TOK, TOK), 1)
    zero = jnp.zeros((64, TOK), BF16)

    def visit(s):
        t = s - straight
        far = jnp.where(lax.rem(t, 2) == 1, z - straight - (t + 1) // 2, t // 2 - 1)
        return jnp.where(s <= straight, z - s, far)

    def load_keys(blocks):
        for i, k in enumerate(blocks):
            block = kv[k]
            t = block.T
            cols = slice(i * TOK, (i + 1) * TOK)
            ktile[0, :, cols] = jnp.concatenate([t[:64], zero], 0)
            ktile[1, :, cols] = jnp.concatenate([zero, t[:64]], 0)
            vtile[0, :, cols] = jnp.concatenate([t[64:], zero], 0)
            vtile[1, :, cols] = jnp.concatenate([zero, t[64:]], 0)
            rolled = pltpu.roll(block.astype(F32), 64, 1).astype(BF16)
            none = jnp.zeros_like(block)
            kcat[i * TOK : (i + 1) * TOK, :] = jnp.where(lane2 < 64, block, none)
            kcat[2 * TOK + i * TOK : 2 * TOK + (i + 1) * TOK, :] = jnp.where(lane2 >= 64, rolled, none)

    def run_tile(blocks, first):
        load_keys(blocks)
        dkvt[...] = jnp.zeros((TOK, 2 * TOK), F32)
        cks = [jnp.concatenate([ck[k, h : h + 1, :] for k in blocks], 1) for h in range(4)]
        if first:
            col = lax.broadcasted_iota(jnp.int32, (TQ, 2 * TOK), 1)
            other = jnp.where(even, -1, 1 << 20)
            key_pos = jnp.where(col < TOK, b * TOK + col, other)

        def rows(t, _):
            q = qg[pl.ds(tb * t, tb)].reshape(TQ, 256)
            do = dg[pl.ds(tb * t, tb)].reshape(TQ, 256)
            ps, dss = [], []
            if first:
                allowed = key_pos <= lax.broadcasted_iota(jnp.int32, (TQ, 2 * TOK), 0) + t * TQ
            for h in range(4):
                lanes = slice(128 * (h // 2), 128 * (h // 2) + 128)
                s = jnp.dot(q[:, lanes], ktile[h % 2], preferred_element_type=F32)
                ra = rowb[h, pl.ds(tb * t, tb)].reshape(TQ, TOK)
                rd = rowb[4 + h, pl.ds(tb * t, tb)].reshape(TQ, TOK)
                logits = (s * c1 + jnp.concatenate([ra, ra], 1)) - cks[h]
                if first:
                    logits = jnp.where(allowed, logits, NEG_LARGE)
                p = jnp.exp2(logits)
                dp = jnp.dot(do[:, lanes], vtile[h % 2], preferred_element_type=F32)
                ds = p * (dp - jnp.concatenate([rd, rd], 1))
                ps.append(p.astype(BF16))
                dss.append(ds.astype(BF16))
            dkvt[:64] += jnp.dot(qtl[t], jnp.concatenate(dss, 0), preferred_element_type=F32)
            dkvt[64:] += jnp.dot(dtl[t], jnp.concatenate(ps, 0), preferred_element_type=F32)
            for g in range(2):
                pair = jnp.concatenate([dss[2 * g], dss[2 * g + 1]], 1)
                add = jnp.dot(pair, kcat[...], preferred_element_type=F32)
                dq[pl.ds(tb * t, tb), :, 128 * g : 128 * g + 128] += add.reshape(tb, TOK, TOK)
            return 0

        lax.fori_loop(0, nt, rows, 0)

    def wait_keys(k):
        remote(kv.at[k], kv.at[k], k_s.at[0], k_r.at[k], sib).wait_recv()

    def g_copy(k):
        return remote(gsend.at[k], grecv.at[z], g_s.at[k], g_r.at[z], at(z=k))

    def pass_on(i, k):
        gsend[k] = dkvt[:, i * TOK : (i + 1) * TOK].T.astype(BF16)
        g_copy(k).start()

    second = jnp.where(even, visit(1), z)

    @pl.when(even)
    def _():
        wait_keys(second)

    run_tile((z, second), True)
    own[...] = dkvt[:, :TOK].T

    @pl.when(even)
    def _():
        pass_on(1, second)

    def later(i, _):
        blocks = (visit(2 * i - skip), visit(2 * i + 1 - skip))
        for k in blocks:
            wait_keys(k)
        run_tile(blocks, False)
        for j, k in enumerate(blocks):
            pass_on(j, k)
        return 0

    lax.fori_loop(1, (z + 2) // 2, later, 0)

    for r in xorder + [0]:
        k = lax.rem(x + r, nx)
        slot = 2 * k + 1 - c
        remote(dq.at[slot], dqd.at[k], d_s.at[k], d_r.at[k], sib).start()
    for r in xorder:
        k = lax.rem(x + r, nx)
        remote(dqd.at[k], dqd.at[k], d_s.at[k], d_r.at[k], sib).wait_recv()
        dqs[k] = ((dq[2 * k + c] + dqd[k]) * 0.125).astype(BF16)
        remote(dqs.at[k], dqr.at[x], e_s.at[k], e_r.at[x], at(x=k)).start()
    remote(dqd.at[x], dqd.at[x], d_s.at[x], d_r.at[x], sib).wait_recv()
    total = (dq[b] + dqd[x]) * 0.125

    def collect(k, _):
        remote(grecv.at[k], grecv.at[k], g_s.at[0], g_r.at[k], sib).wait_recv()
        own[...] += grecv[k].astype(F32)
        return 0

    lax.fori_loop(z + 1, nz, collect, 0)
    scale = jnp.where(lane2 < 64, 0.125, 1.0)
    dkv_out[...] = (own[...] * scale).astype(BF16)

    for r in xorder:
        k = lax.rem(x + r, nx)
        remote(dqr.at[k], dqr.at[k], e_s.at[k], e_r.at[k], sib).wait_recv()
        total = total + dqr[k].astype(F32)
    dq_out[...] = total.astype(BF16)

    for r in range(1, ny):
        k = lax.rem(y + r, ny)
        remote(norm_out.at[k], norm_out.at[k], n_s.at[r], n_r.at[k], sib).wait_recv()

    for r in range(1, nb):
        remote(aux.at[b], aux.at[b], aux_s.at[r], aux_r.at[b], xc(r)).wait_send()
    for i in range(2):
        for k in range(nx):
            remote(q_ref, qg.at[b], f_s.at[i, k], q_r.at[i, b], sib).wait_send()
        for r in range(1, nx):
            remote(q_ref, qg.at[b], q_s.at[i, r], q_r.at[i, b], sib).wait_send()
    for r in range(1, ny):
        remote(norm_ref, norm_out.at[y], n_s.at[r], n_r.at[y], yy(r)).wait_send()
    for r in zorder:
        peer = lax.rem(z + r, nz)

        @pl.when(peer > z)
        def _():
            k_copy(r, peer).wait_send()
            ka_copy(r, peer).wait_send()

    def sent(k, _):
        g_copy(k).wait_send()
        return 0

    lax.fori_loop(0, z, sent, 0)
    for k in range(nx):
        remote(dq.at[0], dqd.at[k], d_s.at[k], d_r.at[k], sib).wait_send()
    for r in range(1, nx):
        k = lax.rem(x + r, nx)
        remote(dqs.at[k], dqr.at[x], e_s.at[k], e_r.at[x], at(x=k)).wait_send()


def attention(nz, nx, ny, q, k, gate, lse, out, do, norm):
    nb = 2 * nx
    vmem = pl.BlockSpec(memory_space=pltpu.VMEM)
    dma = pltpu.SemaphoreType.DMA
    nt = nb * TOK // TQ
    width = norm.shape[1]
    scratch = [
        pltpu.VMEM((nb, TOK, 256), BF16),
        pltpu.VMEM((nb, TOK, 256), BF16),
        pltpu.VMEM((nz, TOK, TOK), BF16),
        pltpu.VMEM((nb, 16, TOK), F32),
        pltpu.VMEM((nb, 8, TOK), F32),
        pltpu.VMEM((nz, 8, TOK), F32),
        pltpu.VMEM((nz, 8, TOK), F32),
        pltpu.VMEM((8, nb, TOK, TOK), F32),
        pltpu.VMEM((nt, 64, 4 * TQ), BF16),
        pltpu.VMEM((nt, 64, 4 * TQ), BF16),
        pltpu.VMEM((2, TOK, 2 * TOK), BF16),
        pltpu.VMEM((2, TOK, 2 * TOK), BF16),
        pltpu.VMEM((4 * TOK, TOK), BF16),
        pltpu.VMEM((nb, TOK, 256), F32),
        pltpu.VMEM((TOK, 2 * TOK), F32),
        pltpu.VMEM((TOK, TOK), F32),
        pltpu.VMEM((nz, TOK, TOK), BF16),
        pltpu.VMEM((nz, TOK, TOK), BF16),
        pltpu.VMEM((nx, TOK, 256), F32),
        pltpu.VMEM((nx, TOK, 256), BF16),
        pltpu.VMEM((nx, TOK, 256), BF16),
        dma((nb,)), dma((nb,)),
        dma((2, nx)), dma((2, nb)), dma((2, nx)),
        dma((nz,)), dma((nz,)), dma((nz,)), dma((nz,)),
        dma((ny,)), dma((ny,)),
        dma((nz,)), dma((nz,)),
        dma((nx,)), dma((nx,)), dma((nx,)), dma((nx,)),
    ]
    return pl.pallas_call(
        functools.partial(attention_kernel, nz, nx, ny),
        out_shape=(
            jax.ShapeDtypeStruct((TOK, 256), BF16),
            jax.ShapeDtypeStruct((TOK, TOK), BF16),
            jax.ShapeDtypeStruct((ny, TOK, width), BF16),
        ),
        in_specs=[vmem] * 7,
        out_specs=(vmem, vmem, vmem),
        scratch_shapes=scratch,
        compiler_params=pltpu.CompilerParams(
            collective_id=0, has_side_effects=True, vmem_limit_bytes=48 * 1024 * 1024
        ),
        name="attention",
    )(q, k, gate, lse, out, do, norm)


def weight_kernel(nz, nx, ny, norm_ref, kg_ref, w_out, part, half, hrecv, mid, msend, mrecv, last, lrecv,
                  h_s, h_r, m_s, m_r, l_s, l_r):
    z, x, c = (lax.axis_index(a) for a in SP)
    sib = at(c=1 - c)
    width = norm_ref.shape[2]
    rows = ny * width // (2 * nx * nz)

    peers = [sib] + [at(x=lax.rem(x + r, nx)) for r in range(1, nx)]
    peers += [at(z=lax.rem(z + r, nz)) for r in range(1, nz)]

    kg = kg_ref[...]
    per = nx * rows * 2
    for k in range(ny):
        w = jnp.dot(norm_ref[k].T, kg, preferred_element_type=F32)
        zs = width // per
        w = w.reshape(zs, nx, 2, rows, 64)
        for cc in range(2):
            part[cc, :, k * zs : (k + 1) * zs] = jnp.swapaxes(w[:, :, cc], 0, 1)
    greet(peers)

    remote(part.at[1 - c], hrecv, h_s, h_r, sib).start()
    remote(part.at[1 - c], hrecv, h_s, h_r, sib).wait_recv()
    order = [r for r in range(1, nx)]
    for r in order:
        k = lax.rem(x + r, nx)
        msend[k] = part[c, k] + hrecv[k]
        remote(msend.at[k], mrecv.at[x], m_s.at[k], m_r.at[x], at(x=k)).start()
    mid[...] = part[c, x] + hrecv[x]
    for r in order:
        k = lax.rem(x + r, nx)
        remote(mrecv.at[k], mrecv.at[k], m_s.at[k], m_r.at[k], sib).wait_recv()
        mid[...] += mrecv[k]
    for r in range(1, nz):
        k = lax.rem(z + r, nz)
        remote(mid.at[k], lrecv.at[z], l_s.at[k], l_r.at[z], at(z=k)).start()
    total = mid[z]
    for r in range(1, nz):
        k = lax.rem(z + r, nz)
        remote(lrecv.at[k], lrecv.at[k], l_s.at[k], l_r.at[k], sib).wait_recv()
        total = total + lrecv[k]
    w_out[...] = total

    remote(part.at[1 - c], hrecv, h_s, h_r, sib).wait_send()
    for r in order:
        k = lax.rem(x + r, nx)
        remote(msend.at[k], mrecv.at[x], m_s.at[k], m_r.at[x], at(x=k)).wait_send()
    for r in range(1, nz):
        k = lax.rem(z + r, nz)
        remote(mid.at[k], lrecv.at[z], l_s.at[k], l_r.at[z], at(z=k)).wait_send()


def weight(nz, nx, ny, norm, kg):
    vmem = pl.BlockSpec(memory_space=pltpu.VMEM)
    dma = pltpu.SemaphoreType.DMA
    rows = ny * norm.shape[2] // (2 * nx * nz)
    return pl.pallas_call(
        functools.partial(weight_kernel, nz, nx, ny),
        out_shape=jax.ShapeDtypeStruct((rows, 64), F32),
        in_specs=[vmem] * 2,
        out_specs=vmem,
        scratch_shapes=[
            pltpu.VMEM((2, nx, nz, rows, 64), F32),
            pltpu.VMEM((8, 128), F32),
            pltpu.VMEM((nx, nz, rows, 64), F32),
            pltpu.VMEM((nz, rows, 64), F32),
            pltpu.VMEM((nx, nz, rows, 64), F32),
            pltpu.VMEM((nx, nz, rows, 64), F32),
            pltpu.VMEM((8, 128), F32),
            pltpu.VMEM((nz, rows, 64), F32),
            dma, dma,
            dma((nx,)), dma((nx,)),
            dma((nz,)), dma((nz,)),
        ],
        compiler_params=pltpu.CompilerParams(
            collective_id=1, has_side_effects=True, vmem_limit_bytes=32 * 1024 * 1024
        ),
        name="weight",
    )(norm, kg)


def body(nz, nx, ny, queries, keys, values, log_gate, log_sum, output, cotangent, normed):
    stacked = jnp.concatenate([keys, values], axis=1)
    query_grad, pair, rows = attention(nz, nx, ny, queries, stacked, log_gate, log_sum, output, cotangent, normed)
    key_grad, value_grad = pair[:, :64], pair[:, 64:]
    weight_grad = weight(nz, nx, ny, rows, key_grad)
    return (query_grad, key_grad, value_grad, weight_grad)


def solution(mesh):
    nz, nx, ny = mesh.shape["sp"] // 8, 4, mesh.shape["tp"]
    split = Mesh(mesh.devices.reshape(nz, nx, 2, ny), SP + ("tp",))
    placed = (
        P(SP, "tp"), P(SP, "tp"), P(SP, "tp"), P("tp", SP),
        P("tp", SP), P(SP, "tp"), P(SP, "tp"), P(SP, "tp"),
    )
    return jax.shard_map(
        functools.partial(body, nz, nx, ny),
        mesh=split,
        in_specs=placed,
        out_specs=(P(SP, "tp"), P(SP, "tp"), P(SP, "tp"), P(SP, "tp")),
        check_vma=False,
    )
```

time: 641 us -> 123 us (0.19)
  waiting for transfers between devices: 288 us -> 0 us
  starting transfers between devices: 248 us -> 0 us
  Pallas kernels: 0 us -> 115 us
  blocking collectives: 40.2 us -> 0 us
  other arithmetic: 16.9 us -> 0.09 us
  between operations: 15.6 us -> 0.7 us
  loops' own time: 12.9 us -> 0 us
    ppermute x69 -> x0, starting transfers between devices: 244 us -> none  [the longest x37 137 us: shifted(): return lax.ppermute(x, axis, pairs)]
    ppermute x69 -> x0, waiting for transfers between devices: 160 us -> none  [the longest x32 150 us: shifted_2(): return lax.ppermute(x, axis, [(i, (i + by) % size) for i in range(size)])]
    reduce_scatter x3 -> x0, waiting for transfers between devices: 128 us -> none  [own_block(): tiles = lax.psum_scatter(tiles, axes[k], scatter_dimension=0, tiled=True)]
    pallas_call x0 -> x2, Pallas kernels: none -> 115 us  [the longest x1 73.4 us: attention(): pl.pallas_call(functools.partial(attention_kernel, nz, nx, ny), out_shape...]
    all_gather x1 -> x0, blocking collectives: 25.2 us -> none  [entering(): pieces = lax.all_gather(total, axis)]
    unnamed x2 -> x0, blocking collectives: 15 us -> none
    add x51 -> x0, other arithmetic: 14.2 us -> none  [the longest x16 12.5 us: turn(): key_pos = blocks[:, None] * tokens + jnp.arange(tokens)[None, :]]
    another operation x17 -> x0, loops' own time: 12.9 us -> none  [the longest x1 12.3 us: body(): finished = lax.fori_loop(0, turns, turn, start_state)]
  transfers between devices with their start and end apart: 73 -> 0, of which waited for: 25 -> 0; matrix products, arithmetic and copies ran while one was open for 1% -> 0% of each run, Pallas kernels for 0% -> 0%
where the time goes in v1:
time: 123 us
  Pallas kernels  115 us (93%)
  local copies, waits for them, and re-layouts  7.46 us (6%)
    pallas_call x1, Pallas kernels, attention(): pl.pallas_call(functools.partial(attention_kernel, nz, nx, ny), out_shape...  73.4 us
    pallas_call x1, Pallas kernels, weight(): pl.pallas_call(functools.partial(weight_kernel, nz, nx, ny), out_shape=ja...  41.1 us
    unnamed x18, local copies, waits for them, and re-layouts  7.38 us

profile of v1, /device:TPU:1, one launch (start us, length us, event | category | flops | bytes accessed | tf_op | source)
XLA Modules:
  0.0 122.8 jit_solution(2328984827982840869)
XLA Ops:
  0.6 0.0 copy-start
  0.6 0.9 copy.12
  1.5 0.0 copy-start.1
  1.5 0.9 copy.13
  2.4 0.1 pad_maximum_fusion.k_ref
  2.5 0.0 copy-done
  2.5 0.0 copy-done.1
  2.5 0.0 copy-start.2
  2.5 0.8 copy-done.2
  3.3 0.0 copy-start.3
  3.3 0.8 copy-done.3
  4.2 0.0 copy-start.4
  4.2 0.7 copy-done.4
  4.9 0.0 copy-start.5
  4.9 0.7 copy-done.5
  5.5 73.4 %attention.1 = (bf16[128,256]{1,0:T(8,128)(2,1)S(1)}, bf16[128,128]{1,0:T(8,128)(2,1)S(1)}, bf16[4,128,512]{2,1,0:T(8,128)(2,1)S(1)}) custom-call(bf16[128,256]{1,0:T(8,128)(2,1)S(1)} %copy-done.1, bf16[128,128]{1,0:T(8,128)(2,1)S(1)} %pad_maximum_fusion.k_ref, f32[4,128]{1,0:T(4,128)S(1)} %copy-done.4, f32[4,128]{1,0:T(4,128)S(1)} %copy-done.5, ...), custom_call_target="tpu_custom_call" | custom-call | tf_op jit(solution)/shard_map/attention/pallas_call | solution.py:364
  79.0 0.1 fusion
  79.1 41.1 %weight.1 = f32[16,64]{1,0:T(8,128)S(1)} custom-call(bf16[4,128,512]{2,1,0:T(8,128)(2,1)S(1)} %get-tuple-element.9.norm_ref, bf16[128,64]{1,0:T(8,128)(2,1)S(1)} %get-tuple-element.15.kg_ref), custom_call_target="tpu_custom_call" | custom-call | tf_op jit(solution)/shard_map/weight/pallas_call | solution.py:436
  120.2 0.7 copy.15
  120.9 0.7 copy.14
  121.6 0.6 copy.18
  122.2 0.6 copy.19
Async XLA Ops:
  0.6 1.8 %copy-start = (bf16[128,512]{1,0:T(8,128)(2,1)S(1)}, bf16[128,512]{1,0:T(8,128)(2,1)}, u32[]{:S(2)}) copy-start(bf16[128,512]{1,0:T(8,128)(2,1)} %norm_ref.1) | copy-start | bytes 393220
  1.5 1.0 copy-start.1
  2.5 0.8 copy-start.2
  3.3 0.8 copy-start.3
  4.2 0.7 copy-start.4
  4.9 0.7 copy-start.5

commit v2 on v1

v2 whole, which is shorter than its diff:
```python
import functools
import math

import jax
import jax.numpy as jnp
from jax import lax
from jax.experimental import pallas as pl
from jax.experimental.pallas import tpu as pltpu
from jax.sharding import Mesh
from jax.sharding import PartitionSpec as P

SP = ("sp_0", "sp_1", "sp_2")
MESH = pl.DeviceIdType.MESH
LOG2E = math.log2(math.e)
NEG_LARGE = -1e30
TOK = 128
TQ = 256
F32, BF16 = jnp.float32, jnp.bfloat16


def at(z=None, x=None, c=None, y=None):
    named = {"sp_0": z, "sp_1": x, "sp_2": c, "tp": y}
    return {k: v for k, v in named.items() if v is not None}


def remote(src, dst, send, recv, peer):
    return pltpu.make_async_remote_copy(
        src_ref=src, dst_ref=dst, send_sem=send, recv_sem=recv, device_id=peer, device_id_type=MESH
    )


def attention_kernel(
    nz, nx, ny,
    q_in, k_in, v_in, gate_in, lse_in, out_in, do_in, norm_in,
    dq_out, k_out, v_out, w_out,
    q_ref, k_half, v_half, gate_ref, lse_ref, out_ref, do_ref, norm_ref, k_ref,
    qg, dg, kv, aux, stat, kaux, ck, rowb, qtl, dtl, ktile, vtile, kcat, dq, dkvt, own,
    gsend, grecv, dqd, dqs, dqr, norm_all, part, hrecv, msend, mrecv, mid, lrecv,
    i_s, aux_s, aux_r, q_s, q_r, f_s, k_s, k_r, ka_s, ka_r, n_s, n_r, g_s, g_r, d_s, d_r, e_s, e_r,
    h_s, h_r, m_s, m_r, l_s, l_r,
):
    z, x, c, y = (lax.axis_index(a) for a in ("sp_0", "sp_1", "sp_2", "tp"))
    nb = 2 * nx
    b = 2 * x + c
    sib = at(c=1 - c)
    c1 = 0.125 * LOG2E
    tb = TQ // TOK
    nt = nb // tb

    def xc(r):
        k = lax.rem(b + r, nb)
        return at(x=k // 2, c=lax.rem(k, 2))

    def zz(r):
        return at(z=lax.rem(z + r, nz))

    def yy(r):
        return at(y=lax.rem(y + r, ny))

    loads = [
        pltpu.make_async_copy(src, dst, i_s.at[i])
        for i, (src, dst) in enumerate((
            (gate_in, gate_ref), (lse_in, lse_ref), (out_in, out_ref), (do_in, do_ref),
            (k_in, k_half), (v_in, v_half), (q_in, q_ref), (norm_in, norm_ref),
        ))
    ]
    for load in loads:
        load.start()
    peers = [xc(r) for r in range(1, nb)] + [zz(r) for r in range(1, nz)] + [yy(r) for r in range(1, ny)]
    barrier = pltpu.get_barrier_semaphore()
    for peer in peers:
        pl.semaphore_signal(barrier, inc=1, device_id=peer, device_id_type=MESH)
    for load in loads:
        load.wait()

    lane = lax.broadcasted_iota(jnp.int32, (4, TOK), 1)
    run = gate_ref[...]
    for s in (1, 2, 4, 8, 16, 32, 64):
        run = run + jnp.where(lane >= s, pltpu.roll(run, s, 1), 0.0)
    prod = (out_ref[...].astype(F32) * do_ref[...].astype(F32)).T
    aux[b, 0:4, :] = run
    aux[b, 4:8, :] = run - lse_ref[...]
    aux[b, 8:12, :] = jnp.sum(prod.reshape(4, 64, TOK), axis=1)
    aux[b, 12:16, :] = jnp.zeros((4, TOK), F32)
    k_ref[...] = jnp.concatenate([k_half[...], v_half[...]], axis=0).T
    kv[z] = k_ref[...]
    qg[b] = q_ref[...]
    dg[b] = do_ref[...]
    norm_all[y] = norm_ref[...]

    pl.semaphore_wait(barrier, len(peers))

    def nearest_first(n):
        pairs = zip(range(1, n // 2 + 1), range(n - 1, n // 2 - 1, -1))
        return list(dict.fromkeys(r for pair in pairs for r in pair))

    xorder, zorder = nearest_first(nx), nearest_first(nz)
    sources = ((q_ref, qg), (do_ref, dg))

    up, down = nz // 2, nz - 1 - nz // 2

    def reach(stage):
        if stage == 0:
            return [(0, d) for d in (1, 2) if d <= up] + [(0, -d) for d in (1, 2) if d <= down]
        ahead = [(-d, 2) for d in (2 * stage - 1, 2 * stage) if d + 2 <= up]
        return ahead + [(d, -2) for d in (2 * stage - 1, 2 * stage) if d + 2 <= down]

    def fresh(stage):
        seen = (2 * stage - 1, 2 * stage)
        return [-d for d in seen if d <= up] + [d for d in seen if d <= down]

    def useful(k, distance, upward):
        return k + distance < nz if upward else k < down - (down - distance) % 2

    def k_wait(stage):
        for offset in fresh(stage):
            k = lax.rem(z + offset + nz, nz)

            @pl.when(useful(k, abs(offset), offset < 0))
            def _():
                remote(kv.at[k], kv.at[k], k_s.at[0], k_r.at[k], sib).wait_recv()

    def k_moves(stage):
        for i, (offset, step) in enumerate(reach(stage)):
            k = lax.rem(z + offset + nz, nz)
            src = k_ref if stage == 0 else kv.at[k]
            copy = remote(src, kv.at[k], k_s.at[4 * stage + i], k_r.at[k], zz(step + nz))
            yield useful(k, abs(offset) + abs(step), step > 0), copy

    def k_send(stage):
        for wanted, copy in k_moves(stage):
            pl.when(wanted)(copy.start)

    def k_pass(stage):
        k_wait(stage)
        if stage < stages:
            k_send(stage)

    stages = (nz // 2 + 1) // 2
    def ka_copy(peer):
        return remote(kaux.at[z], kaux.at[z], ka_s.at[peer], ka_r.at[z], at(z=peer))

    def to_later(copy, steps):
        for r in steps:
            peer = lax.rem(z + r, nz)

            @pl.when(peer > z)
            def _():
                copy(peer).start()

    for r in range(1, nb):
        remote(aux.at[b], aux.at[b], aux_s.at[r], aux_r.at[b], xc(r)).start()
    for i, (src, dst) in enumerate(sources):
        remote(src, dst.at[b], f_s.at[i, x], q_r.at[i, b], sib).start()
    for r in xorder:
        peer = lax.rem(x + r, nx)
        for i, (src, dst) in enumerate(sources):
            remote(src, dst.at[b], q_s.at[i, peer], q_r.at[i, b], at(x=peer)).start()
    k_send(0)

    def prepare(k):
        qt = qg[k].T
        dt = dg[k].T
        stats = jnp.concatenate([stat[k], jnp.zeros((TOK - 8, TOK), F32)], 0).T
        qtl[k] = jnp.concatenate([qt[64 * h : 64 * h + 64] for h in range(4)], 1)
        dtl[k] = jnp.concatenate([dt[64 * h : 64 * h + 64] for h in range(4)], 1)
        for r in range(8):
            rowb[r, k] = jnp.broadcast_to(stats[:, r : r + 1], (TOK, TOK))
        dq[k] = jnp.zeros((TOK, 256), F32)

    for r in range(1, nb):
        k = lax.rem(b + r, nb)
        remote(aux.at[k], aux.at[k], aux_s.at[r], aux_r.at[k], sib).wait_recv()
    before = jnp.zeros((4, TOK), F32)
    mine = jnp.zeros((4, TOK), F32)
    for k in range(nb):
        mine = jnp.where(b == k, before, mine)
        stat[k, 0:4, :] = (aux[k, 4:8, :] + before) * LOG2E
        stat[k, 4:8, :] = aux[k, 8:12, :]
        before = before + jnp.broadcast_to(aux[k, 0:4, TOK - 1 : TOK], (4, TOK))
    kaux[z, 0:4, :] = run + mine
    kaux[z, 4:8, :] = before
    ck[z, 0:4, :] = (run + mine) * LOG2E
    to_later(ka_copy, zorder)
    k_pass(1)
    for r in range(1, ny):
        remote(norm_ref, norm_all.at[y], n_s.at[r], n_r.at[y], yy(r)).start()
    prepare(b)

    def arrived(k):
        for i, (_, dst) in enumerate(sources):
            remote(dst.at[k], dst.at[k], q_s.at[i, 0], q_r.at[i, k], sib).wait_recv()

    arrived(2 * x + 1 - c)
    prepare(2 * x + 1 - c)
    for r in xorder:
        other = lax.rem(x + nx - r, nx)
        k = 2 * other + c
        arrived(k)
        for i, (_, dst) in enumerate(sources):
            remote(dst.at[k], dst.at[k], f_s.at[i, other], q_r.at[i, k], sib).start()
        prepare(k)
    for r in xorder:
        k = 2 * lax.rem(x + nx - r, nx) + 1 - c
        arrived(k)
        prepare(k)

    def offsets(i, total):
        k = z - 1 - i
        remote(kaux.at[k], kaux.at[k], ka_s.at[0], ka_r.at[k], sib).wait_recv()
        total = total + kaux[k, 4:8, :]
        ck[k, 0:4, :] = (kaux[k, 0:4, :] - total) * LOG2E
        return total

    even = lax.rem(z, 2) == 1
    skip = jnp.where(even, 0, 1)
    straight = jnp.minimum(nz - 1 - z, z)

    def visit(s):
        t = s - straight
        far = jnp.where(lax.rem(t, 2) == 1, z - straight - (t + 1) // 2, t // 2 - 1)
        return jnp.where(s <= straight, z - s, far)

    near = 6 - skip

    def turn(s):
        return visit(jnp.where(s < near, s, z + near - s))

    lane2 = lax.broadcasted_iota(jnp.int32, (TOK, TOK), 1)
    zero = jnp.zeros((64, TOK), BF16)

    def load_keys(blocks):
        for i, k in enumerate(blocks):
            block = kv[k]
            t = block.T
            cols = slice(i * TOK, (i + 1) * TOK)
            ktile[0, :, cols] = jnp.concatenate([t[:64], zero], 0)
            ktile[1, :, cols] = jnp.concatenate([zero, t[:64]], 0)
            vtile[0, :, cols] = jnp.concatenate([t[64:], zero], 0)
            vtile[1, :, cols] = jnp.concatenate([zero, t[64:]], 0)
            rolled = pltpu.roll(block.astype(F32), 64, 1).astype(BF16)
            none = jnp.zeros_like(block)
            kcat[i * TOK : (i + 1) * TOK, :] = jnp.where(lane2 < 64, block, none)
            kcat[2 * TOK + i * TOK : 2 * TOK + (i + 1) * TOK, :] = jnp.where(lane2 >= 64, rolled, none)

    def run_tile(blocks, first, between):
        load_keys(blocks)
        dkvt[...] = jnp.zeros((TOK, 2 * TOK), F32)
        cks = [jnp.concatenate([ck[k, h : h + 1, :] for k in blocks], 1) for h in range(4)]
        if first:
            col = lax.broadcasted_iota(jnp.int32, (TQ, 2 * TOK), 1)
            other = jnp.where(even, -1, 1 << 20)
            key_pos = jnp.where(col < TOK, b * TOK + col, other)

        def rows(t, _):
            q = qg[pl.ds(tb * t, tb)].reshape(TQ, 256)
            do = dg[pl.ds(tb * t, tb)].reshape(TQ, 256)
            ps, dss = [], []
            if first:
                allowed = key_pos <= lax.broadcasted_iota(jnp.int32, (TQ, 2 * TOK), 0) + t * TQ
            for h in range(4):
                lanes = slice(128 * (h // 2), 128 * (h // 2) + 128)
                s = jnp.dot(q[:, lanes], ktile[h % 2], preferred_element_type=F32)
                ra = rowb[h, pl.ds(tb * t, tb)].reshape(TQ, TOK)
                rd = rowb[4 + h, pl.ds(tb * t, tb)].reshape(TQ, TOK)
                logits = (s * c1 + jnp.concatenate([ra, ra], 1)) - cks[h]
                if first:
                    logits = jnp.where(allowed, logits, NEG_LARGE)
                p = jnp.exp2(logits)
                dp = jnp.dot(do[:, lanes], vtile[h % 2], preferred_element_type=F32)
                ds = p * (dp - jnp.concatenate([rd, rd], 1))
                ps.append(p.astype(BF16))
                dss.append(ds.astype(BF16))

            def by_block(parts):
                return jnp.concatenate([p[j * TOK : (j + 1) * TOK] for j in range(tb) for p in parts], 0)

            qt = jnp.concatenate([qtl[tb * t + j] for j in range(tb)], 1)
            dt = jnp.concatenate([dtl[tb * t + j] for j in range(tb)], 1)
            dkvt[:64] += jnp.dot(qt, by_block(dss), preferred_element_type=F32)
            dkvt[64:] += jnp.dot(dt, by_block(ps), preferred_element_type=F32)
            for g in range(2):
                pair = jnp.concatenate([dss[2 * g], dss[2 * g + 1]], 1)
                add = jnp.dot(pair, kcat[...], preferred_element_type=F32)
                dq[pl.ds(tb * t, tb), :, 128 * g : 128 * g + 128] += add.reshape(tb, TOK, TOK)
            return 0

        lax.fori_loop(0, nt // 2, rows, 0)
        between()
        lax.fori_loop(nt // 2, nt, rows, 0)

    def g_copy(k):
        return remote(gsend.at[k], grecv.at[z], g_s.at[k], g_r.at[z], at(z=k))

    def pass_on(i, k):
        gsend[k] = dkvt[:, i * TOK : (i + 1) * TOK].T.astype(BF16)
        g_copy(k).start()

    second = jnp.where(even, visit(1), z)
    early = jnp.minimum(z, 1)
    total = lax.fori_loop(0, early, offsets, jnp.zeros((4, TOK), F32))

    run_tile((z, second), True, lambda: k_pass(2) if stages > 1 else None)
    own[...] = dkvt[:, :TOK].T

    @pl.when(even)
    def _():
        pass_on(1, second)

    def later(i, carry):
        known, total = carry
        last = 2 * i + 1 - skip
        need = jnp.where(last <= jnp.minimum(straight, near - 1), last, z)
        total = lax.fori_loop(known, need, offsets, total)
        blocks = (turn(last - 1), turn(last))
        if stages > 3:
            pl.when(i == 3)(functools.partial(k_wait, 4))
        run_tile(blocks, False, lambda: pl.when(i == 1)(lambda: k_pass(3)) if stages > 2 else None)
        for j, k in enumerate(blocks):
            pass_on(j, k)
        return (need, total)

    lax.fori_loop(1, (z + 2) // 2, later, (early, total))
    if stages > 2:
        pl.when((z + 2) // 2 < 2)(functools.partial(k_pass, 3))
    if stages > 3:
        pl.when((z + 2) // 2 < 4)(functools.partial(k_wait, 4))

    for r in xorder + [0]:
        k = lax.rem(x + r, nx)
        slot = 2 * k + 1 - c
        remote(dq.at[slot], dqd.at[k], d_s.at[k], d_r.at[k], sib).start()
    for r in xorder:
        k = lax.rem(x + r, nx)
        remote(dqd.at[k], dqd.at[k], d_s.at[k], d_r.at[k], sib).wait_recv()
        dqs[k] = ((dq[2 * k + c] + dqd[k]) * 0.125).astype(BF16)
        remote(dqs.at[k], dqr.at[x], e_s.at[k], e_r.at[x], at(x=k)).start()
    remote(dqd.at[x], dqd.at[x], d_s.at[x], d_r.at[x], sib).wait_recv()

    for r in range(1, ny):
        k = lax.rem(y + r, ny)
        remote(norm_all.at[k], norm_all.at[k], n_s.at[r], n_r.at[k], sib).wait_recv()

    def collect(k, _):
        remote(grecv.at[k], grecv.at[k], g_s.at[0], g_r.at[k], sib).wait_recv()
        own[...] += grecv[k].astype(F32)
        return 0

    lax.fori_loop(z + 1, nz, collect, 0)
    kg = (own[:, :64] * 0.125).astype(BF16)
    both = own[...].T
    k_out[...] = (both[:64] * 0.125).astype(BF16)
    v_out[...] = both[64:].astype(BF16)

    width = norm_in.shape[1]
    rows16 = w_out.shape[0]
    half = rows16 // 2
    zs = width // (nb * rows16)
    for k in range(ny):
        w = jnp.dot(norm_all[k].T, kg, preferred_element_type=F32).reshape(zs * nb, rows16, 64)
        w = jnp.concatenate([w[:, :half], w[:, half:]], 2).reshape(zs, nx, 2, half, TOK)
        for cc in range(2):
            for xx in range(nx):
                part[cc, xx, k * zs : (k + 1) * zs] = w[:, xx, cc]
    h_copy = remote(part.at[1 - c], hrecv, h_s, h_r, sib)
    h_copy.start()
    h_copy.wait_recv()
    for r in xorder:
        k = lax.rem(x + r, nx)
        msend[k] = (part[c, k] + hrecv[k]).reshape(nz * half, TOK).astype(BF16)
        remote(msend.at[k], mrecv.at[x], m_s.at[k], m_r.at[x], at(x=k)).start()
    sums = part[c, x] + hrecv[x]
    for r in xorder:
        k = lax.rem(x + r, nx)
        remote(mrecv.at[k], mrecv.at[k], m_s.at[k], m_r.at[k], sib).wait_recv()
        sums = sums + mrecv[k].astype(F32).reshape(nz, half, TOK)
    mid[...] = sums

    def l_copy(k):
        return remote(mid.at[k], lrecv.at[z], l_s.at[k], l_r.at[z], at(z=k))

    for r in zorder[::-1]:
        l_copy(lax.rem(z + r, nz)).start()

    grad = (dq[b] + dqd[x]) * 0.125
    for r in xorder:
        k = lax.rem(x + r, nx)
        remote(dqr.at[k], dqr.at[k], e_s.at[k], e_r.at[k], sib).wait_recv()
        grad = grad + dqr[k].astype(F32)
    dq_out[...] = grad.astype(BF16)

    w_sum = mid[z]
    for r in zorder:
        k = lax.rem(z + r, nz)
        remote(lrecv.at[k], lrecv.at[k], l_s.at[k], l_r.at[k], sib).wait_recv()
        w_sum = w_sum + lrecv[k]
    w_out[...] = jnp.concatenate([w_sum[:, :64], w_sum[:, 64:]], 0)

    for r in range(1, nb):
        remote(aux.at[b], aux.at[b], aux_s.at[r], aux_r.at[b], xc(r)).wait_send()
    for i, (src, dst) in enumerate(sources):
        for k in range(nx):
            remote(src, dst.at[b], f_s.at[i, k], q_r.at[i, b], sib).wait_send()
        for r in xorder:
            peer = lax.rem(x + r, nx)
            remote(src, dst.at[b], q_s.at[i, peer], q_r.at[i, b], at(x=peer)).wait_send()
    for r in range(1, ny):
        remote(norm_ref, norm_all.at[y], n_s.at[r], n_r.at[y], yy(r)).wait_send()

    for stage in range(stages):
        for wanted, copy in k_moves(stage):
            pl.when(wanted)(copy.wait_send)

    def sent_on(k, _):
        ka_copy(k).wait_send()
        return 0

    lax.fori_loop(z + 1, nz, sent_on, 0)

    def sent_back(k, _):
        g_copy(k).wait_send()
        return 0

    lax.fori_loop(0, z, sent_back, 0)
    for k in range(nx):
        remote(dq.at[0], dqd.at[k], d_s.at[k], d_r.at[k], sib).wait_send()
    h_copy.wait_send()
    for r in xorder:
        k = lax.rem(x + r, nx)
        remote(dqs.at[k], dqr.at[x], e_s.at[k], e_r.at[x], at(x=k)).wait_send()
        remote(msend.at[k], mrecv.at[x], m_s.at[k], m_r.at[x], at(x=k)).wait_send()
    for r in zorder:
        l_copy(lax.rem(z + r, nz)).wait_send()


def attention(nz, nx, ny, *arrays):
    nb = 2 * nx
    vmem = pl.BlockSpec(memory_space=pltpu.VMEM)
    anywhere = pl.BlockSpec(memory_space=pltpu.HBM)
    dma = pltpu.SemaphoreType.DMA
    width = arrays[-1].shape[1]
    rows = ny * width // (nb * nz)
    bf, f32 = (lambda *s: pltpu.VMEM(s, BF16)), (lambda *s: pltpu.VMEM(s, F32))
    scratch = [
        bf(TOK, 256), bf(64, TOK), bf(64, TOK), f32(4, TOK), f32(4, TOK), bf(TOK, 256), bf(TOK, 256),
        bf(TOK, width), bf(TOK, TOK),
        bf(nb, TOK, 256), bf(nb, TOK, 256), bf(nz, TOK, TOK),
        f32(nb, 16, TOK), f32(nb, 8, TOK), f32(nz, 8, TOK), f32(nz, 8, TOK),
        f32(8, nb, TOK, TOK), bf(nb, 64, 4 * TOK), bf(nb, 64, 4 * TOK),
        bf(2, TOK, 2 * TOK), bf(2, TOK, 2 * TOK), bf(4 * TOK, TOK),
        f32(nb, TOK, 256), f32(TOK, 2 * TOK), f32(TOK, TOK),
        bf(nz, TOK, TOK), bf(nz, TOK, TOK),
        f32(nx, TOK, 256), bf(nx, TOK, 256), bf(nx, TOK, 256),
        bf(ny, TOK, width),
        f32(2, nx, nz, rows // 2, TOK), f32(nx, nz, rows // 2, TOK),
        bf(nx, nz * rows // 2, TOK), bf(nx, nz * rows // 2, TOK),
        f32(nz, rows // 2, TOK), f32(nz, rows // 2, TOK),
        dma((8,)),
        dma((nb,)), dma((nb,)),
        dma((2, nx)), dma((2, nb)), dma((2, nx)),
        dma((16,)), dma((nz,)), dma((nz,)), dma((nz,)),
        dma((ny,)), dma((ny,)),
        dma((nz,)), dma((nz,)),
        dma((nx,)), dma((nx,)), dma((nx,)), dma((nx,)),
        dma, dma,
        dma((nx,)), dma((nx,)),
        dma((nz,)), dma((nz,)),
    ]
    return pl.pallas_call(
        functools.partial(attention_kernel, nz, nx, ny),
        out_shape=(
            jax.ShapeDtypeStruct((TOK, 256), BF16),
            jax.ShapeDtypeStruct((64, TOK), BF16),
            jax.ShapeDtypeStruct((64, TOK), BF16),
            jax.ShapeDtypeStruct((rows, 64), F32),
        ),
        in_specs=[anywhere] * 8,
        out_specs=(vmem, vmem, vmem, vmem),
        scratch_shapes=scratch,
        compiler_params=pltpu.CompilerParams(
            collective_id=0, has_side_effects=True, vmem_limit_bytes=67043328
        ),
        name="attention",
    )(*arrays)


def finish_kernel(n, *refs):
    src, dst, held, sem = refs[:n], refs[n : 2 * n], refs[2 * n : 3 * n], refs[-1]
    loads = [pltpu.make_async_copy(src[i], held[i], sem.at[0, i]) for i in range(n)]
    stores = [pltpu.make_async_copy(held[i], dst[i], sem.at[1, i]) for i in range(n)]
    for load in loads:
        load.start()
    for load, store in zip(loads, stores):
        load.wait()
        store.start()
    for store in stores:
        store.wait()


def finish(*arrays):
    n = len(arrays)
    hbm = pl.BlockSpec(memory_space=pltpu.HBM)
    return pl.pallas_call(
        functools.partial(finish_kernel, n),
        out_shape=tuple(jax.ShapeDtypeStruct(a.shape, a.dtype) for a in arrays),
        in_specs=[hbm] * n,
        out_specs=(hbm,) * n,
        scratch_shapes=[pltpu.VMEM(a.shape, a.dtype) for a in arrays] + [pltpu.SemaphoreType.DMA((2, n))],
        compiler_params=pltpu.CompilerParams(vmem_limit_bytes=67043328),
        name="finish",
    )(*arrays)


def body(nz, nx, ny, q, k, v, *arrays):
    query_grad, key_grad, value_grad, weight_grad = finish(*attention(nz, nx, ny, q, k.T, v.T, *arrays))
    return (query_grad, key_grad.T, value_grad.T, weight_grad)


def solution(mesh):
    nz, nx, ny = mesh.shape["sp"] // 8, 4, mesh.shape["tp"]
    split = Mesh(mesh.devices.reshape(nz, nx, 2, ny), SP + ("tp",))
    placed = (
        P(SP, "tp"), P(SP, "tp"), P(SP, "tp"), P("tp", SP),
        P("tp", SP), P(SP, "tp"), P(SP, "tp"), P(SP, "tp"),
    )
    return jax.shard_map(
        functools.partial(body, nz, nx, ny),
        mesh=split,
        in_specs=placed,
        out_specs=(P(SP, "tp"), P(SP, "tp"), P(SP, "tp"), P(SP, "tp")),
        check_vma=False,
    )
```

time: 123 us -> 80.5 us (0.65)
  Pallas kernels: 115 us -> 79.6 us
  local copies, waits for them, and re-layouts: 7.46 us -> 0 us
    pallas_call x1, Pallas kernels: 41.1 us -> 1.55 us  [finish(): pl.pallas_call(functools.partial(finish_kernel, n), out_shape=tuple((jax....]
    unnamed x18 -> x0, local copies, waits for them, and re-layouts: 7.38 us -> none
    pallas_call x1, Pallas kernels: 73.4 us -> 78.1 us  [attention(): pl.pallas_call(functools.partial(attention_kernel, nz, nx, ny), out_shape...]
where the time goes in v2:
time: 80.5 us; the launch traced here: 80.3 us
  Pallas kernels  79.6 us (99%)
    pallas_call x1, Pallas kernels, attention(): pl.pallas_call(functools.partial(attention_kernel, nz, nx, ny), out_shape...  78.1 us

profile of v2, /device:TPU:1, one launch (start us, length us, event | category | flops | bytes accessed | tf_op | source)
XLA Modules:
  0.0 80.3 jit_solution(4276442367354167949)
XLA Ops:
  0.6 78.1 %attention.1 = (bf16[128,256]{1,0:T(8,128)(2,1)}, bf16[64,128]{1,0:T(8,128)(2,1)}, bf16[64,128]{1,0:T(8,128)(2,1)}, f32[16,64]{1,0:T(8,128)}) custom-call(bf16[128,256]{1,0:T(8,128)(2,1)} %q_in.1, bf16[64,128]{1,0:T(8,128)(2,1)} %bitcast.4, bf16[64,128]{1,0:T(8,128)(2,1)} %bitcast.5, f32[4,128]{1,0:T(4,128)} %gate_in.1, f32[4,128]{1,0:T(4,128)} %lse_in.1, ...), custom_call_target="tpu_custom_call" | custom-call | tf_op jit(solution)/shard_map/attention/pallas_call | solution.py:469
  78.7 1.5 %finish.1 = (bf16[128,256]{1,0:T(8,128)(2,1)}, bf16[64,128]{1,0:T(8,128)(2,1)}, bf16[64,128]{1,0:T(8,128)(2,1)}, f32[16,64]{1,0:T(8,128)}) custom-call(bf16[128,256]{1,0:T(8,128)(2,1)} %get-tuple-element.12.refs_0_, bf16[64,128]{1,0:T(8,128)(2,1)} %get-tuple-element.13.refs_1_, bf16[64,128]{1,0:T(8,128)(2,1)} %get-tuple-element.14.refs_2_, ...), custom_call_target="tpu_custom_call" | custom-call | tf_op jit(solution)/shard_map/finish/pallas_call | solution.py:503

commit v3 on v2

--- a/solution.py
+++ b/solution.py
@@ -14,7 +14,7 @@
 LOG2E = math.log2(math.e)
 NEG_LARGE = -1e30
 TOK = 128
-TQ = 256
+TQ = 512
 F32, BF16 = jnp.float32, jnp.bfloat16
 
 
@@ -32,12 +32,13 @@
 def attention_kernel(
     nz, nx, ny,
     q_in, k_in, v_in, gate_in, lse_in, out_in, do_in, norm_in,
+    dq_hbm, k_hbm, v_hbm, w_hbm,
     dq_out, k_out, v_out, w_out,
     q_ref, k_half, v_half, gate_ref, lse_ref, out_ref, do_ref, norm_ref, k_ref,
     qg, dg, kv, aux, stat, kaux, ck, rowb, qtl, dtl, ktile, vtile, kcat, dq, dkvt, own,
     gsend, grecv, dqd, dqs, dqr, norm_all, part, hrecv, msend, mrecv, mid, lrecv,
-    i_s, aux_s, aux_r, q_s, q_r, f_s, k_s, k_r, ka_s, ka_r, n_s, n_r, g_s, g_r, d_s, d_r, e_s, e_r,
-    h_s, h_r, m_s, m_r, l_s, l_r,
+    i_s, aux_s, aux_r, q_s, q_r, w_s, f_s, k_s, k_r, ka_s, ka_r, n_s, n_r, g_s, g_r, d_s, d_r, e_s, e_r,
+    h_s, h_r, m_s, m_r, l_s, l_r, o_s,
 ):
     z, x, c, y = (lax.axis_index(a) for a in ("sp_0", "sp_1", "sp_2", "tp"))
     nb = 2 * nx
@@ -101,7 +102,7 @@
 
     def reach(stage):
         if stage == 0:
-            return [(0, d) for d in (1, 2) if d <= up] + [(0, -d) for d in (1, 2) if d <= down]
+            return [(0, d) for d in range(1, 5) if d <= up] + [(0, -d) for d in range(1, 5) if d <= down]
         ahead = [(-d, 2) for d in (2 * stage - 1, 2 * stage) if d + 2 <= up]
         return ahead + [(d, -2) for d in (2 * stage - 1, 2 * stage) if d + 2 <= down]
 
@@ -124,7 +125,7 @@
         for i, (offset, step) in enumerate(reach(stage)):
             k = lax.rem(z + offset + nz, nz)
             src = k_ref if stage == 0 else kv.at[k]
-            copy = remote(src, kv.at[k], k_s.at[4 * stage + i], k_r.at[k], zz(step + nz))
+            copy = remote(src, kv.at[k], k_s.at[4 * stage + i if stage else i], k_r.at[k], zz(step + nz))
             yield useful(k, abs(offset) + abs(step), step > 0), copy
 
     def k_send(stage):
@@ -133,7 +134,7 @@
 
     def k_pass(stage):
         k_wait(stage)
-        if stage < stages:
+        if 1 < stage < stages:
             k_send(stage)
 
     stages = (nz // 2 + 1) // 2
@@ -152,10 +153,14 @@
         remote(aux.at[b], aux.at[b], aux_s.at[r], aux_r.at[b], xc(r)).start()
     for i, (src, dst) in enumerate(sources):
         remote(src, dst.at[b], f_s.at[i, x], q_r.at[i, b], sib).start()
-    for r in xorder:
-        peer = lax.rem(x + r, nx)
-        for i, (src, dst) in enumerate(sources):
-            remote(src, dst.at[b], q_s.at[i, peer], q_r.at[i, b], at(x=peer)).start()
+    def q_moves():
+        for r in xorder:
+            peer = lax.rem(x + r, nx)
+            for i, (src, dst) in enumerate(sources[:1] if 2 * r == nx == 4 else sources):
+                yield remote(src, dst.at[b], q_s.at[i, peer], q_r.at[i, b], at(x=peer))
+
+    for copy in q_moves():
+        copy.start()
     k_send(0)
 
     def prepare(k):
@@ -182,7 +187,6 @@
     kaux[z, 4:8, :] = before
     ck[z, 0:4, :] = (run + mine) * LOG2E
     to_later(ka_copy, zorder)
-    k_pass(1)
     for r in range(1, ny):
         remote(norm_ref, norm_all.at[y], n_s.at[r], n_r.at[y], yy(r)).start()
     prepare(b)
@@ -191,19 +195,39 @@
         for i, (_, dst) in enumerate(sources):
             remote(dst.at[k], dst.at[k], q_s.at[i, 0], q_r.at[i, k], sib).wait_recv()
 
+    def share(chip):
+        k = 2 * chip + c
+        arrived(k)
+        for i, (_, dst) in enumerate(sources):
+            remote(dst.at[k], dst.at[k], f_s.at[i, chip], q_r.at[i, k], sib).start()
+
+    def relay():
+        k = 2 * lax.rem(x + 1, nx) + c
+        return remote(dg.at[k], dg.at[k], w_s, q_r.at[1, k], at(x=lax.rem(x + nx - 1, nx)))
+
+    def complete(chip):
+        prepare(2 * chip + c)
+        arrived(2 * chip + 1 - c)
+        prepare(2 * chip + 1 - c)
+
     arrived(2 * x + 1 - c)
     prepare(2 * x + 1 - c)
-    for r in xorder:
-        other = lax.rem(x + nx - r, nx)
-        k = 2 * other + c
-        arrived(k)
-        for i, (_, dst) in enumerate(sources):
-            remote(dst.at[k], dst.at[k], f_s.at[i, other], q_r.at[i, k], sib).start()
-        prepare(k)
-    for r in xorder:
-        k = 2 * lax.rem(x + nx - r, nx) + 1 - c
-        arrived(k)
-        prepare(k)
+    odd = lax.rem(x, 2)
+    if nx > 1:
+        share(lax.rem(x + 1, nx))
+    if nx == 4:
+        relay().start()
+        share(lax.rem(x + nx - 1, nx))
+    if nx > 1:
+        complete(x + 1 - 2 * odd)
+
+    def rest():
+        if nx == 4:
+            complete(lax.rem(x + 3 - 2 * odd, nx))
+            share(lax.rem(x + 2, nx))
+            complete(lax.rem(x + 2, nx))
+        if stages > 1:
+            k_pass(2)
 
     def offsets(i, total):
         k = z - 1 - i
@@ -221,10 +245,13 @@
         far = jnp.where(lax.rem(t, 2) == 1, z - straight - (t + 1) // 2, t // 2 - 1)
         return jnp.where(s <= straight, z - s, far)
 
-    near = 6 - skip
+    held = jnp.where(z >= max(3 * nz // 4, 7), 2, 0)
+    near = 8 - skip
+    last_wait = jnp.where(even & (held == 0), 3, 4)
 
     def turn(s):
-        return visit(jnp.where(s < near, s, z + near - s))
+        ahead = jnp.where(s < near, s + held, z + near - s)
+        return visit(jnp.where(s > z - held, z + 2 - skip - s, ahead))
 
     lane2 = lax.broadcasted_iota(jnp.int32, (TOK, TOK), 1)
     zero = jnp.zeros((64, TOK), BF16)
@@ -243,7 +270,7 @@
             kcat[i * TOK : (i + 1) * TOK, :] = jnp.where(lane2 < 64, block, none)
             kcat[2 * TOK + i * TOK : 2 * TOK + (i + 1) * TOK, :] = jnp.where(lane2 >= 64, rolled, none)
 
-    def run_tile(blocks, first, between):
+    def run_tile(blocks, first, between=None):
         load_keys(blocks)
         dkvt[...] = jnp.zeros((TOK, 2 * TOK), F32)
         cks = [jnp.concatenate([ck[k, h : h + 1, :] for k in blocks], 1) for h in range(4)]
@@ -285,9 +312,12 @@
                 dq[pl.ds(tb * t, tb), :, 128 * g : 128 * g + 128] += add.reshape(tb, TOK, TOK)
             return 0
 
-        lax.fori_loop(0, nt // 2, rows, 0)
-        between()
-        lax.fori_loop(nt // 2, nt, rows, 0)
+        if between is None:
+            lax.fori_loop(0, nt, rows, 0)
+        else:
+            lax.fori_loop(0, nt // 2, lambda i, _: rows(x // 2, 0), 0)
+            between()
+            lax.fori_loop(nt // 2, nt, lambda i, _: rows(nt // 2 - x // 2 if nt == 2 else i, 0), 0)
 
     def g_copy(k):
         return remote(gsend.at[k], grecv.at[z], g_s.at[k], g_r.at[z], at(z=k))
@@ -296,11 +326,13 @@
         gsend[k] = dkvt[:, i * TOK : (i + 1) * TOK].T.astype(BF16)
         g_copy(k).start()
 
+    k_pass(1)
+
     second = jnp.where(even, visit(1), z)
     early = jnp.minimum(z, 1)
     total = lax.fori_loop(0, early, offsets, jnp.zeros((4, TOK), F32))
 
-    run_tile((z, second), True, lambda: k_pass(2) if stages > 1 else None)
+    run_tile((z, second), True, rest)
     own[...] = dkvt[:, :TOK].T
 
     @pl.when(even)
@@ -310,21 +342,23 @@
     def later(i, carry):
         known, total = carry
         last = 2 * i + 1 - skip
-        need = jnp.where(last <= jnp.minimum(straight, near - 1), last, z)
+        need = jnp.where((last <= jnp.minimum(straight, near - 1)) & (held == 0), last, z)
         total = lax.fori_loop(known, need, offsets, total)
         blocks = (turn(last - 1), turn(last))
+        if stages > 2:
+            pl.when(i == 2)(functools.partial(k_pass, 3))
         if stages > 3:
-            pl.when(i == 3)(functools.partial(k_wait, 4))
-        run_tile(blocks, False, lambda: pl.when(i == 1)(lambda: k_pass(3)) if stages > 2 else None)
+            pl.when(i == last_wait)(functools.partial(k_wait, 4))
+        run_tile(blocks, False)
         for j, k in enumerate(blocks):
             pass_on(j, k)
         return (need, total)
 
     lax.fori_loop(1, (z + 2) // 2, later, (early, total))
     if stages > 2:
-        pl.when((z + 2) // 2 < 2)(functools.partial(k_pass, 3))
+        pl.when((z + 2) // 2 < 3)(functools.partial(k_pass, 3))
     if stages > 3:
-        pl.when((z + 2) // 2 < 4)(functools.partial(k_wait, 4))
+        pl.when((z + 2) // 2 <= last_wait)(functools.partial(k_wait, 4))
 
     for r in xorder + [0]:
         k = lax.rem(x + r, nx)
@@ -351,6 +385,10 @@
     both = own[...].T
     k_out[...] = (both[:64] * 0.125).astype(BF16)
     v_out[...] = both[64:].astype(BF16)
+    held_out = ((k_out, k_hbm), (v_out, v_hbm), (dq_out, dq_hbm), (w_out, w_hbm))
+    stores = [pltpu.make_async_copy(src, dst, o_s.at[i]) for i, (src, dst) in enumerate(held_out)]
+    stores[0].start()
+    stores[1].start()
 
     width = norm_in.shape[1]
     rows16 = w_out.shape[0]
@@ -388,6 +426,7 @@
         remote(dqr.at[k], dqr.at[k], e_s.at[k], e_r.at[k], sib).wait_recv()
         grad = grad + dqr[k].astype(F32)
     dq_out[...] = grad.astype(BF16)
+    stores[2].start()
 
     w_sum = mid[z]
     for r in zorder:
@@ -395,20 +434,22 @@
         remote(lrecv.at[k], lrecv.at[k], l_s.at[k], l_r.at[k], sib).wait_recv()
         w_sum = w_sum + lrecv[k]
     w_out[...] = jnp.concatenate([w_sum[:, :64], w_sum[:, 64:]], 0)
+    stores[3].start()
 
     for r in range(1, nb):
         remote(aux.at[b], aux.at[b], aux_s.at[r], aux_r.at[b], xc(r)).wait_send()
     for i, (src, dst) in enumerate(sources):
         for k in range(nx):
             remote(src, dst.at[b], f_s.at[i, k], q_r.at[i, b], sib).wait_send()
-        for r in xorder:
-            peer = lax.rem(x + r, nx)
-            remote(src, dst.at[b], q_s.at[i, peer], q_r.at[i, b], at(x=peer)).wait_send()
+    for copy in q_moves():
+        copy.wait_send()
+    if nx == 4:
+        relay().wait_send()
     for r in range(1, ny):
         remote(norm_ref, norm_all.at[y], n_s.at[r], n_r.at[y], yy(r)).wait_send()
 
     for stage in range(stages):
-        for wanted, copy in k_moves(stage):
+        for wanted, copy in k_moves(stage) if stage != 1 else ():
             pl.when(wanted)(copy.wait_send)
 
     def sent_on(k, _):
@@ -431,17 +472,19 @@
         remote(msend.at[k], mrecv.at[x], m_s.at[k], m_r.at[x], at(x=k)).wait_send()
     for r in zorder:
         l_copy(lax.rem(z + r, nz)).wait_send()
+    for store in stores:
+        store.wait()
 
 
 def attention(nz, nx, ny, *arrays):
     nb = 2 * nx
-    vmem = pl.BlockSpec(memory_space=pltpu.VMEM)
     anywhere = pl.BlockSpec(memory_space=pltpu.HBM)
     dma = pltpu.SemaphoreType.DMA
     width = arrays[-1].shape[1]
     rows = ny * width // (nb * nz)
     bf, f32 = (lambda *s: pltpu.VMEM(s, BF16)), (lambda *s: pltpu.VMEM(s, F32))
     scratch = [
+        bf(TOK, 256), bf(64, TOK), bf(64, TOK), f32(rows, 64),
         bf(TOK, 256), bf(64, TOK), bf(64, TOK), f32(4, TOK), f32(4, TOK), bf(TOK, 256), bf(TOK, 256),
         bf(TOK, width), bf(TOK, TOK),
         bf(nb, TOK, 256), bf(nb, TOK, 256), bf(nz, TOK, TOK),
@@ -457,7 +500,7 @@
         f32(nz, rows // 2, TOK), f32(nz, rows // 2, TOK),
         dma((8,)),
         dma((nb,)), dma((nb,)),
-        dma((2, nx)), dma((2, nb)), dma((2, nx)),
+        dma((2, nx)), dma((2, nb)), dma, dma((2, nx)),
         dma((16,)), dma((nz,)), dma((nz,)), dma((nz,)),
         dma((ny,)), dma((ny,)),
         dma((nz,)), dma((nz,)),
@@ -465,6 +508,7 @@
         dma, dma,
         dma((nx,)), dma((nx,)),
         dma((nz,)), dma((nz,)),
+        dma((4,)),
     ]
     return pl.pallas_call(
         functools.partial(attention_kernel, nz, nx, ny),
@@ -475,7 +519,7 @@
             jax.ShapeDtypeStruct((rows, 64), F32),
         ),
         in_specs=[anywhere] * 8,
-        out_specs=(vmem, vmem, vmem, vmem),
+        out_specs=(anywhere,) * 4,
         scratch_shapes=scratch,
         compiler_params=pltpu.CompilerParams(
             collective_id=0, has_side_effects=True, vmem_limit_bytes=67043328

time: 80.5 us -> 77.1 us (0.958)
  Pallas kernels: 79.6 us -> 76.1 us
    pallas_call x1, Pallas kernels: 78.1 us -> 74.5 us  [attention(): pl.pallas_call(functools.partial(attention_kernel, nz, nx, ny), out_shape...]
where the time goes in v3:
time: 77.1 us; the launch traced here: 76.7 us
  Pallas kernels  76.1 us (99%)
    pallas_call x1, Pallas kernels, attention(): pl.pallas_call(functools.partial(attention_kernel, nz, nx, ny), out_shape...  74.5 us
    pallas_call x1, Pallas kernels, finish(): pl.pallas_call(functools.partial(finish_kernel, n), out_shape=tuple((jax....  1.55 us

profile of v3, /device:TPU:1, one launch (start us, length us, event | category | flops | bytes accessed | tf_op | source)
XLA Modules:
  0.0 76.7 jit_solution(7463874926576180165)
XLA Ops:
  0.6 74.5 %attention.1 = (bf16[128,256]{1,0:T(8,128)(2,1)}, bf16[64,128]{1,0:T(8,128)(2,1)}, bf16[64,128]{1,0:T(8,128)(2,1)}, f32[16,64]{1,0:T(8,128)}) custom-call(bf16[128,256]{1,0:T(8,128)(2,1)} %q_in.1, bf16[64,128]{1,0:T(8,128)(2,1)} %bitcast.4, bf16[64,128]{1,0:T(8,128)(2,1)} %bitcast.5, f32[4,128]{1,0:T(4,128)} %gate_in.1, f32[4,128]{1,0:T(4,128)} %lse_in.1, ...), custom_call_target="tpu_custom_call" | custom-call | tf_op jit(solution)/shard_map/attention/pallas_call | solution.py:513
  75.2 1.5 %finish.1 = (bf16[128,256]{1,0:T(8,128)(2,1)}, bf16[64,128]{1,0:T(8,128)(2,1)}, bf16[64,128]{1,0:T(8,128)(2,1)}, f32[16,64]{1,0:T(8,128)}) custom-call(bf16[128,256]{1,0:T(8,128)(2,1)} %get-tuple-element.12.refs_0_, bf16[64,128]{1,0:T(8,128)(2,1)} %get-tuple-element.13.refs_1_, bf16[64,128]{1,0:T(8,128)(2,1)} %get-tuple-element.14.refs_2_, ...), custom_call_target="tpu_custom_call" | custom-call | tf_op jit(solution)/shard_map/finish/pallas_call | solution.py:547

commit v4 on v3

--- a/solution.py
+++ b/solution.py
@@ -529,16 +529,12 @@
 
 
 def finish_kernel(n, *refs):
-    src, dst, held, sem = refs[:n], refs[n : 2 * n], refs[2 * n : 3 * n], refs[-1]
-    loads = [pltpu.make_async_copy(src[i], held[i], sem.at[0, i]) for i in range(n)]
-    stores = [pltpu.make_async_copy(held[i], dst[i], sem.at[1, i]) for i in range(n)]
-    for load in loads:
-        load.start()
-    for load, store in zip(loads, stores):
-        load.wait()
-        store.start()
-    for store in stores:
-        store.wait()
+    sem = refs[-1]
+    copies = [pltpu.make_async_copy(refs[i], refs[n + i], sem.at[i]) for i in range(n)]
+    for copy in copies:
+        copy.start()
+    for copy in copies:
+        copy.wait()
 
 
 def finish(*arrays):
@@ -549,7 +545,7 @@
         out_shape=tuple(jax.ShapeDtypeStruct(a.shape, a.dtype) for a in arrays),
         in_specs=[hbm] * n,
         out_specs=(hbm,) * n,
-        scratch_shapes=[pltpu.VMEM(a.shape, a.dtype) for a in arrays] + [pltpu.SemaphoreType.DMA((2, n))],
+        scratch_shapes=[pltpu.SemaphoreType.DMA((n,))],
         compiler_params=pltpu.CompilerParams(vmem_limit_bytes=67043328),
         name="finish",
     )(*arrays)

time: 77.1 us -> 79.9 us (1.036)
  Pallas kernels: 76.1 us -> 78.9 us
    pallas_call x1, Pallas kernels: 1.55 us -> 4.37 us  [finish(): pl.pallas_call(functools.partial(finish_kernel, n), out_shape=tuple((jax....]
where the time goes in v4:
time: 79.9 us; the launch traced here: 79.5 us
  Pallas kernels  78.9 us (99%)
    pallas_call x1, Pallas kernels, attention(): pl.pallas_call(functools.partial(attention_kernel, nz, nx, ny), out_shape...  74.5 us
    pallas_call x1, Pallas kernels, finish(): pl.pallas_call(functools.partial(finish_kernel, n), out_shape=tuple((jax....  4.37 us

profile of v4, /device:TPU:1, one launch (start us, length us, event | category | flops | bytes accessed | tf_op | source)
XLA Modules:
  0.0 79.5 jit_solution(16189725214293865074)
XLA Ops:
  0.6 74.5 %attention.1 = (bf16[128,256]{1,0:T(8,128)(2,1)}, bf16[64,128]{1,0:T(8,128)(2,1)}, bf16[64,128]{1,0:T(8,128)(2,1)}, f32[16,64]{1,0:T(8,128)}) custom-call(bf16[128,256]{1,0:T(8,128)(2,1)} %q_in.1, bf16[64,128]{1,0:T(8,128)(2,1)} %bitcast.4, bf16[64,128]{1,0:T(8,128)(2,1)} %bitcast.5, f32[4,128]{1,0:T(4,128)} %gate_in.1, f32[4,128]{1,0:T(4,128)} %lse_in.1, ...), custom_call_target="tpu_custom_call" | custom-call | tf_op jit(solution)/shard_map/attention/pallas_call | solution.py:513
  75.2 4.4 %finish.1 = (bf16[128,256]{1,0:T(8,128)(2,1)}, bf16[64,128]{1,0:T(8,128)(2,1)}, bf16[64,128]{1,0:T(8,128)(2,1)}, f32[16,64]{1,0:T(8,128)}) custom-call(bf16[128,256]{1,0:T(8,128)(2,1)} %get-tuple-element.12.refs_0_, bf16[64,128]{1,0:T(8,128)(2,1)} %get-tuple-element.13.refs_1_, bf16[64,128]{1,0:T(8,128)(2,1)} %get-tuple-element.14.refs_2_, ...), custom_call_target="tpu_custom_call" | custom-call | tf_op jit(solution)/shard_map/finish/pallas_call | solution.py:543
